TPU v7x, 256 devices: a whole 4x4x8 slice. The times are simulated.
256 devices in a mesh: sp: 32 (over z, y), tp: 8 (over x, core).
Axes of the slice: x: 4, y: 4, z: 8, core: 2. Of those that a mesh axis runs over, the one named last changes fastest.
Arguments:
- latent: bfloat16 [16384, 2048], P(('sp', 'tp')), may hold values from -6 to 6
- context: bfloat16 [512, 2048], P('sp'), may hold values from -6 to 6
- condition: float32 [2048], replicated, may hold values from -6 to 6
- context_condition: float32 [2048], replicated, may hold values from -6 to 6
- norm_gain: float32 [2048], replicated, may hold values from 0.1 to 1.9
- shift_weight: bfloat16 [2048, 2048], P('sp', 'tp'), may hold values from -0.21875 to 0.21875
- scale_weight: bfloat16 [2048, 2048], P('sp', 'tp'), may hold values from -0.21875 to 0.21875
- gate_weight: bfloat16 [2048, 2048], P('sp', 'tp'), may hold values from -0.21875 to 0.21875
- query_weight: bfloat16 [2048, 1024], P(None, 'tp'), may hold values from -1 to 1
- key_weight: bfloat16 [2048, 512], P(None, 'tp'), may hold values from -1 to 1
- value_weight: bfloat16 [2048, 512], P(None, 'tp'), may hold values from -0.125 to 0.125
- query_gain: float32 [64], replicated, may hold values from 0.1 to 7.8
- key_gain: float32 [64], replicated, may hold values from 0.1 to 7.8
- output_weight: bfloat16 [1024, 2048], replicated, may hold values from -1 to 1
Outputs:
- updated: bfloat16 [16384, 2048], P(('sp', 'tp'))
All inputs are finite; a program needn't handle non-finite values.
Results may differ from a plain program's by a relative error of at most 0.012.
The roundings to bfloat16 on the way count: a program that leaves them out, or rounds other values in their place, can miss the bound.
Values may be sent and summed in bfloat16 or wider, within the bound.
A program may use at most 64 MiB of HBM per device.

v0:
```python
import math

import jax
import jax.numpy as jnp
from jax import lax
from jax.sharding import Mesh
from jax.sharding import PartitionSpec as P

CHANNEL_SPAN = 64
GRID_W = 64
SP = ("sp_0", "sp_1")
SP_TP = ("sp_0", "sp_1", "tp")


epsilon = 1e-06
rope_base = 10000.0


def from_everyone(array, axis):
    devices = lax.axis_size(axis)
    return lax.all_to_all(
        jnp.broadcast_to(array[None], (devices, *array.shape)), axis, 0, 0, tiled=True
    )


def over_copies(array, axis):
    return from_everyone(array, axis).sum(axis=0)


def packed_total(arrays, axis):
    line, at, done = (jnp.concatenate([a.reshape(-1) for a in arrays]), 0, [])
    total = over_copies(line, axis)
    for a in arrays:
        done.append(total[at : at + a.size].reshape(a.shape))
        at += a.size
    return tuple(done)


def sent_together(arrays, axis, dim, along):
    both = jnp.concatenate(arrays, axis=along)
    result, at, done = (lax.all_gather(both, axis, axis=dim, tiled=True), 0, [])
    for a in arrays:
        done.append(lax.slice_in_dim(result, at, at + a.shape[along], axis=along))
        at += a.shape[along]
    return tuple(done)


def laid_out(pieces, dim):
    dims = list(pieces.shape[1:])
    dims[dim] *= pieces.shape[0]
    return jnp.moveaxis(pieces, 0, dim).reshape(dims)


def collect(array, axis, dim):
    pieces = from_everyone(array, axis)
    return laid_out(pieces, dim)


def whole_of(array, axes, dim):
    result = array
    for number in range(len(axes) - 1, -1, -1):
        result = lax.all_gather(result, axes[number], axis=dim, tiled=True)
    return result


def modulate(tok_rows, norm_gain, shift_row, scale_row):
    wide = tok_rows.astype(jnp.float32)
    normed = wide * lax.rsqrt(jnp.mean(wide * wide, axis=-1, keepdims=True) + epsilon)
    return (normed * norm_gain * (1.0 + scale_row) + shift_row).astype(jnp.bfloat16)


def headnorm(raw, gain, heads):
    field = raw.reshape(raw.shape[0], heads, -1)
    return field * lax.rsqrt(jnp.mean(field * field, axis=-1, keepdims=True) + epsilon) * gain


def rotate(field, places):
    count = field.shape[0]
    heads = field.shape[1]
    quarter = field.shape[2] // 4
    grid_row = (places // GRID_W).astype(jnp.float32)
    grid_col = (places % GRID_W).astype(jnp.float32)
    inverse = rope_base ** (-jnp.arange(quarter, dtype=jnp.float32) / quarter)
    angles = jnp.stack([grid_row[:, None] * inverse, grid_col[:, None] * inverse], axis=1)[:, None]
    cosine = jnp.cos(angles)
    sine = jnp.sin(angles)
    matcher_content_couples = field.reshape(count, heads, 2, 2, quarter)
    first = matcher_content_couples[:, :, :, 0]
    second = matcher_content_couples[:, :, :, 1]
    turned = jnp.stack([first * cosine - second * sine, second * cosine + first * sine], axis=3)
    return turned.reshape(count, heads, 4 * quarter)


def process_probe_group(
    accumulator_carry, probe_entries, matcher_content_couples, similarity_offset
):
    row_peak, row_total, weighted = accumulator_carry
    kv_heads = probe_entries.shape[1]
    head_size = probe_entries.shape[3]
    pair_width = kv_heads * head_size
    matcher_pieces = matcher_content_couples[:, :pair_width].reshape(
        matcher_content_couples.shape[0], kv_heads, head_size
    )
    value_rows = matcher_content_couples[:, pair_width:].reshape(
        matcher_content_couples.shape[0], kv_heads, head_size
    )
    similarity_matrix = (
        jnp.einsum(
            "dmvk,hmk->dmvh", probe_entries, matcher_pieces, preferred_element_type=jnp.float32
        )
        * head_size ** (-0.5)
        + similarity_offset
    )
    new_peak = jnp.maximum(row_peak, jnp.max(similarity_matrix, axis=-1))
    shares = jnp.exp(similarity_matrix - new_peak[..., None])
    shrink = jnp.exp(row_peak - new_peak)
    row_total = row_total * shrink + jnp.sum(shares, axis=-1)
    weighted = weighted * shrink[..., None] + jnp.einsum(
        "qkgn,nkd->qkgd",
        shares.astype(jnp.bfloat16),
        value_rows,
        preferred_element_type=jnp.float32,
    )
    return (new_peak, row_total, weighted)


def group_walker(accumulator_carry, probe_entries, matcher_content_couples, similarity_offset):
    pair_count = matcher_content_couples.shape[0]
    probe_group_total = -(-pair_count // 2048)
    while pair_count % probe_group_total:
        probe_group_total += 1
    if probe_group_total == 1:
        return process_probe_group(
            accumulator_carry, probe_entries, matcher_content_couples, similarity_offset
        )
    group_extent = pair_count // probe_group_total

    def scan_step(inner, slices):
        return (process_probe_group(inner, probe_entries, slices[0], slices[1]), None)

    result, unused = lax.scan(
        scan_step,
        accumulator_carry,
        (
            matcher_content_couples.reshape(
                probe_group_total, group_extent, matcher_content_couples.shape[1]
            ),
            similarity_offset.reshape(probe_group_total, group_extent),
        ),
    )
    return result


def on_device(
    latent,
    context,
    condition,
    context_condition,
    norm_gain,
    shift_weight,
    scale_weight,
    gate_weight,
    query_weight,
    key_weight,
    value_weight,
    query_gain,
    key_gain,
    output_weight,
):
    head_split = lax.axis_size("tp")
    seq_index = lax.axis_index(SP)
    row_slab = shift_weight.shape[0]
    conditions = jnp.stack([condition, context_condition])
    activated = jax.nn.silu(
        lax.dynamic_slice_in_dim(conditions, seq_index * row_slab, row_slab, 1)
    ).astype(jnp.bfloat16)
    part_shift = jnp.dot(activated, shift_weight, preferred_element_type=jnp.float32)
    part_scale = jnp.dot(activated, scale_weight, preferred_element_type=jnp.float32)
    part_gate = jnp.dot(activated, gate_weight, preferred_element_type=jnp.float32)
    sum_shift, sum_scale, sum_gate = packed_total((part_shift, part_scale, part_gate), SP)
    shifts, scales, gates = sent_together((sum_shift, sum_scale, sum_gate), "tp", 1, 0)
    own_rows = latent.shape[0]
    tok_count = own_rows * head_split
    ctx_rows = context.shape[0]
    hidden = modulate(latent, norm_gain, shifts[0], scales[0])
    context_hidden = modulate(context, norm_gain, shifts[1], scales[1])
    q_heads = query_weight.shape[1] // CHANNEL_SPAN
    kv_heads = key_weight.shape[1] // CHANNEL_SPAN
    group_size = q_heads // kv_heads
    q_width = q_heads * CHANNEL_SPAN
    kv_width = kv_heads * CHANNEL_SPAN
    joined_weight = jnp.concatenate([query_weight, key_weight, value_weight], axis=1)
    projected = jnp.dot(collect(hidden, "tp", 0), joined_weight, preferred_element_type=jnp.float32)
    places = seq_index * tok_count + jnp.arange(tok_count, dtype=jnp.int32)
    probe_entries = rotate(headnorm(projected[:, :q_width], query_gain, q_heads), places).astype(
        jnp.bfloat16
    )
    probe_entries = probe_entries.reshape(tok_count, kv_heads, group_size, CHANNEL_SPAN)
    latent_keys = rotate(
        headnorm(projected[:, q_width : q_width + kv_width], key_gain, kv_heads), places
    ).astype(jnp.bfloat16)
    latent_values = projected[:, q_width + kv_width :].astype(jnp.bfloat16)
    own_pairs = jnp.concatenate([latent_keys.reshape(tok_count, kv_width), latent_values], axis=1)
    ctx_projected = jnp.dot(
        context_hidden, joined_weight[:, q_width:], preferred_element_type=jnp.float32
    )
    ctx_keys = (
        headnorm(ctx_projected[:, :kv_width], key_gain, kv_heads)
        .astype(jnp.bfloat16)
        .reshape(ctx_rows, kv_width)
    )
    ctx_pairs = jnp.concatenate(
        [ctx_keys, ctx_projected[:, kv_width:].astype(jnp.bfloat16)], axis=1
    )
    prefix_mapped = math.log(tok_count / (2.0 * ctx_rows))
    stat_shape = (tok_count, kv_heads, group_size)
    start_state = (
        jnp.full(stat_shape, -jnp.inf, jnp.float32),
        jnp.zeros(stat_shape, jnp.float32),
        jnp.zeros(stat_shape + (CHANNEL_SPAN,), jnp.float32),
    )
    ctx_whole = whole_of(ctx_pairs, SP, 0)
    ctx_state = group_walker(
        start_state,
        probe_entries,
        ctx_whole,
        jnp.full((ctx_whole.shape[0],), prefix_mapped, jnp.float32),
    )
    key_piece = whole_of(own_pairs, SP, 0)
    final_state = group_walker(
        ctx_state, probe_entries, key_piece, jnp.zeros((key_piece.shape[0],), jnp.float32)
    )
    row_peak, row_total, weighted = final_state
    attended = (weighted / row_total[..., None]).astype(jnp.bfloat16).reshape(tok_count, q_width)
    branch = jnp.dot(
        lax.all_to_all(attended, "tp", split_axis=0, concat_axis=1, tiled=True),
        output_weight,
        preferred_element_type=jnp.float32,
    )
    return (latent.astype(jnp.float32) + gates[0] * branch).astype(jnp.bfloat16)


def solution(mesh):
    split = Mesh(mesh.devices.reshape(8, 4, mesh.shape["tp"]), ("sp_0", "sp_1", "tp"))
    return jax.shard_map(
        on_device,
        mesh=split,
        in_specs=(
            P(SP_TP, None),
            P(SP, None),
            P(),
            P(),
            P(),
            P(SP, "tp"),
            P(SP, "tp"),
            P(SP, "tp"),
            P(None, "tp"),
            P(None, "tp"),
            P(None, "tp"),
            P(),
            P(),
            P(),
        ),
        out_specs=P(SP_TP, None),
        check_vma=False,
    )
```

profile of v0, /device:TPU:1, one launch (start us, length us, event | category | flops | bytes accessed | tf_op | source)
XLA Modules:
  0.0 218.2 jit_solution(2658111860637024467)
XLA Ops:
  11.0 12.0 %all-to-all-start = ((f32[32,1,1536]{2,1,0:T(1,128)}), f32[32,1,1536]{2,1,0:T(1,128)S(1)}, u32[]{:S(2)}, u32[]{:S(2)}) async-start(f32[32,1,1536]{2,1,0:T(1,128)} %broadcast_in_dim.12), calls=%async_computation | async-start | bytes 393216 | tf_op jit(solution)/shard_map/all_to_all | solution.py:21
  24.1 8.9 %all-to-all-done = f32[32,1,1536]{2,1,0:T(1,128)S(1)} async-done(((f32[32,1,1536]{2,1,0:T(1,128)}), f32[32,1,1536]{2,1,0:T(1,128)S(1)}, u32[]{:S(2)}, u32[]{:S(2)}) %all-to-all-start) | async-done | bytes 196640 | tf_op jit(solution)/shard_map/all_to_all | solution.py:21
  33.2 15.6 %all_gather.15 = f32[6,2048]{1,0:T(8,128)S(1)} all-gather(f32[6,256]{1,0:T(8,128)S(1)} %pad_maximum_fusion.5), channel_id=1, replica_groups=mesh['sp_0'=8,'sp_1'=4,'tp'=8] {'tp'}, dimensions={1}, use_global_device_ids=true | all-gather | bytes 55296 | tf_op jit(solution)/shard_map/all_gather | solution.py:41
  50.5 1.6 broadcast_in_dim.13
  52.1 4.0 %all-to-all-start.1 = ((bf16[8,64,2048]{2,1,0:T(8,128)(2,1)}), bf16[8,64,2048]{2,1,0:T(8,128)(2,1)S(1)}, u32[]{:S(2)}, u32[]{:S(2)}) async-start(bf16[8,64,2048]{2,1,0:T(8,128)(2,1)} %broadcast_in_dim.13), calls=%async_computation.1 | async-start | bytes 4194304 | tf_op jit(solution)/shard_map/all_to_all | solution.py:21
  58.1 24.2 %all-to-all-done.1 = bf16[8,64,2048]{2,1,0:T(8,128)(2,1)S(1)} async-done(((bf16[8,64,2048]{2,1,0:T(8,128)(2,1)}), bf16[8,64,2048]{2,1,0:T(8,128)(2,1)S(1)}, u32[]{:S(2)}, u32[]{:S(2)}) %all-to-all-start.1) | async-done | bytes 2097184 | tf_op jit(solution)/shard_map/all_to_all | solution.py:21
  82.3 2.3 %fusion.25 = f32[512,256]{0,1:T(8,128)S(1)} fusion(bf16[512,2048]{1,0:T(8,128)(2,1)S(1)} %bitcast.172, bf16[2048,64]{1,0:T(8,128)(2,1)} %copy.51, bf16[2048,64]{1,0:T(8,128)(2,1)S(1)} %copy.50, bf16[2048,128]{1,0:T(8,128)(2,1)} %param.24), kind=kOutput, calls=%fused_computation.36 | convolution fusion | flops 540016640 | bytes 3670016 | tf_op jit(solution)/shard_map/dot_general | solution.py:193
  85.1 10.6 %all_gather.18 = bf16[2048,128]{0,1:T(8,128)(2,1)} all-gather(bf16[512,128]{0,1:T(8,128)(2,1)S(1)} %pad_maximum_fusion), channel_id=1, replica_groups=mesh['sp_0'=8,'sp_1'=4,'tp'=8] {'sp_1'}, dimensions={0}, use_global_device_ids=true | all-gather | bytes 655360 | tf_op jit(solution)/shard_map/all_gather | solution.py:62
  96.9 9.1 %all_gather.16 = bf16[64,128]{1,0:T(8,128)(2,1)S(1)} all-gather(bf16[16,128]{1,0:T(8,128)(2,1)S(1)} %pad_maximum_fusion.6), channel_id=1, replica_groups=mesh['sp_0'=8,'sp_1'=4,'tp'=8] {'sp_1'}, dimensions={0}, use_global_device_ids=true | all-gather | bytes 20480 | tf_op jit(solution)/shard_map/all_gather | solution.py:62
  106.0 21.9 %all_gather.17 = bf16[512,128]{1,0:T(8,128)(2,1)S(1)} all-gather(bf16[64,128]{1,0:T(8,128)(2,1)S(1)} %all_gather.16), channel_id=1, replica_groups=mesh['sp_0'=8,'sp_1'=4,'tp'=8] {'sp_0'}, dimensions={0}, use_global_device_ids=true | all-gather | bytes 147456 | tf_op jit(solution)/shard_map/all_gather | solution.py:62
  129.6 19.4 %all-gather.2.cloned.1.call-done = bf16[16384,128]{0,1:T(8,128)(2,1)} async-done(((bf16[2048,128]{0,1:T(8,128)(2,1)}), bf16[16384,128]{0,1:T(8,128)(2,1)}) %all-gather.2.cloned.1.call-update) | async-done | bytes 4194320 | tf_op jit(solution)/shard_map/all_gather | solution.py:62
  149.0 4.7 %copy.78 = bf16[16,8,8,2048]{3,2,0,1:T(8,128)(2,1)} copy(bf16[16,8,8,2048]{3,2,1,0:T(8,128)(2,1)} %bitcast.169) | data formatting | bytes 8388608 | tf_op jit(solution)/shard_map/reshape | solution.py:145
  153.7 43.3 %while.14 = (s32[]{:T(128)}, f32[512,1,2]{0,2,1:T(2,128)S(1)}, f32[512,1,2]{0,2,1:T(2,128)S(1)}, f32[512,1,2,64]{0,3,2,1:T(8,128)S(1)}, bf16[8,2048,128]{1,2,0:T...) while((s32[]{:T(128)}, f32[512,1,2]{0,2,1:T(2,128)S(1)}, f32[512,1,2]{0,2,1:T(2,128)S(1)}, ...), condition=%wide.region_11.12_spmd, body=%wide.region_8.11_spmd.sunk | while | flops 553782272 | bytes 27459672 | solution.py:141
  156.2 1.6 fusion.91
  161.6 1.6 fusion.91
  167.0 1.6 fusion.91
  172.4 1.6 fusion.91
  177.8 1.6 fusion.91
  179.4 1.4 fusion.90
  183.2 1.6 fusion.91
  188.6 1.6 fusion.91
  194.0 1.6 fusion.91
  197.4 10.1 %all_to_all.30 = bf16[8,64,128]{2,1,0:T(8,128)(2,1)S(1)} all-to-all(bf16[8,64,128]{2,1,0:T(8,128)(2,1)S(1)} %copy.56), channel_id=1, replica_groups=mesh['sp_0'=8,'sp_1'=4,'tp'=8] {'tp'}, dimensions={0} | all-to-all | bytes 262144 | tf_op jit(solution)/shard_map/all_to_all | solution.py:236
  207.5 3.8 %fusion.17 = bf16[64,2048]{1,0:T(8,128)(2,1)} fusion(bf16[1024,2048]{1,0:T(8,128)(2,1)} %param.29, bf16[64,2048]{1,0:T(8,128)(2,1)S(1)} %copy-done.1, f32[2048]{0:T(1024)S(1)} %bitcast.184, bf16[8,64,128]{2,1,0:T(8,128)(2,1)S(1)} %all_to_all.30), kind=kOutput, calls=%fused_computation.22 | convolution fusion | flops 268959744 | bytes 4857856 | tf_op jit(solution)/shard_map/dot_general | solution.py:235
  (127 shorter events, 42.1 us)
Async XLA Ops:
  6.5 0.8 copy-start
  11.0 22.0 %all-to-all-start = ((f32[32,1,1536]{2,1,0:T(1,128)}), f32[32,1,1536]{2,1,0:T(1,128)S(1)}, u32[]{:S(2)}, u32[]{:S(2)}) async-start(f32[32,1,1536]{2,1,0:T(1,128)} %broadcast_in_dim.12), calls=%async_computation | async-start | bytes 393216 | tf_op jit(solution)/shard_map/all_to_all | solution.py:21
  52.1 4.0 %copy-start.3 = (bf16[2048,64]{0,1:T(8,128)(2,1)S(1)}, bf16[2048,64]{0,1:T(8,128)(2,1)}, u32[]{:S(2)}) copy-start(bf16[2048,64]{0,1:T(8,128)(2,1)} %param.25) | copy-start | bytes 786436
  52.1 4.3 %copy-start.2 = (bf16[2048,64]{0,1:T(8,128)(2,1)S(1)}, bf16[2048,64]{0,1:T(8,128)(2,1)}, u32[]{:S(2)}) copy-start(bf16[2048,64]{0,1:T(8,128)(2,1)} %param.26) | copy-start | bytes 786436
  52.1 30.2 %all-to-all-start.1 = ((bf16[8,64,2048]{2,1,0:T(8,128)(2,1)}), bf16[8,64,2048]{2,1,0:T(8,128)(2,1)S(1)}, u32[]{:S(2)}, u32[]{:S(2)}) async-start(bf16[8,64,2048]{2,1,0:T(8,128)(2,1)} %broadcast_in_dim.13), calls=%async_computation.1 | async-start | bytes 4194304 | tf_op jit(solution)/shard_map/all_to_all | solution.py:21
  56.1 92.9 %all-gather.2.cloned.1.call-start = ((), (), s32[]{:S(2)}) async-start(), calls=%async_computation.3 | async-start | bytes 4718592 | tf_op jit(solution)/shard_map/all_gather | solution.py:62
  82.3 2.4 %copy-start.9 = (f32[64]{0:T(128)S(1)}, f32[64]{0:T(128)}, u32[]{:S(2)}) copy-start(f32[64]{0:T(128)} %param.28) | copy-start | bytes 772
  82.3 2.5 %copy-start.5 = (f32[512,1,1,1,16]{0,4,3,2,1:T(8,128)S(1)}, f32[512,1,1,1,16]{0,4,3,2,1:T(8,128)}, u32[]{:S(2)}) copy-start(f32[512,1,1,1,16]{0,4,3,2,1:T(8,128)} %get-tuple-element.105) | copy-start | bytes 98308
  84.5 11.2 %copy-start.11 = (f32[64]{0:T(128)S(1)}, f32[64]{0:T(128)}, u32[]{:S(2)}) copy-start(f32[64]{0:T(128)} %param.27) | copy-start | bytes 772
  84.6 11.5 %copy-start.6 = (bf16[16,2048]{1,0:T(8,128)(2,1)S(1)}, bf16[16,2048]{1,0:T(8,128)(2,1)}, u32[]{:S(2)}) copy-start(bf16[16,2048]{1,0:T(8,128)(2,1)} %param.17) | copy-start | bytes 196612
  84.6 11.7 %copy-start.4 = (bf16[2048,64]{0,1:T(8,128)(2,1)S(1)}, bf16[2048,64]{0,1:T(8,128)(2,1)}, u32[]{:S(2)}) copy-start(bf16[2048,64]{0,1:T(8,128)(2,1)} %param.25) | copy-start | bytes 786436
  84.6 11.6 %copy-start.7 = (f32[2048]{0:T(1024)S(1)}, f32[2048]{0:T(1024)}, u32[]{:S(2)}) copy-start(f32[2048]{0:T(1024)} %param.20) | copy-start | bytes 24580
  84.6 11.6 %copy-start.8 = (f32[1,2048]{1,0:T(1,128)S(1)}, f32[1,2048]{1,0:T(1,128)}, u32[]{:S(2)}) copy-start(f32[1,2048]{1,0:T(1,128)} %get-tuple-element.93) | copy-start | bytes 24580
  84.6 12.1 %copy-start.10 = (f32[64]{0:T(128)S(1)}, f32[64]{0:T(128)}, u32[]{:S(2)}) copy-start(f32[64]{0:T(128)} %param.28) | copy-start | bytes 772
  153.7 53.8 %copy-start.1 = (bf16[64,2048]{1,0:T(8,128)(2,1)S(1)}, bf16[64,2048]{1,0:T(8,128)(2,1)}, u32[]{:S(2)}) copy-start(bf16[64,2048]{1,0:T(8,128)(2,1)} %param.16) | copy-start | bytes 786436
Sparse Core Ops, SparseCore 0:
  95.9 53.0 all-gather.1
where the time goes:
time: 219 us; the launch traced here: 218 us
  blocking collectives  67.3 us (31%)
  waiting for transfers between devices  52.4 us (24%)
  matrix products  33.1 us (15%)
  local copies, waits for them, and re-layouts  18.5 us (8%)
  other arithmetic  16.7 us (8%)
  starting transfers between devices  16 us (7%)
  between operations  13.7 us (6%)
    all_gather x3, blocking collectives, whole_of(): result = lax.all_gather(result, axes[number], axis=dim, tiled=True)  41.6 us
    all_to_all x2, waiting for transfers between devices, from_everyone(): lax.all_to_all(jnp.broadcast_to(array[None], (devices, *array.shape)), ax...  33 us
    all_gather x1, waiting for transfers between devices, whole_of(): result = lax.all_gather(result, axes[number], axis=dim, tiled=True)  19.4 us
    all_to_all x2, starting transfers between devices, from_everyone(): lax.all_to_all(jnp.broadcast_to(array[None], (devices, *array.shape)), ax...  16 us
    all_gather x1, blocking collectives, sent_together(): result, at, done = (lax.all_gather(both, axis, axis=dim, tiled=True), 0, [])  15.6 us
    dot_general x9, matrix products, process_probe_group(): jnp.einsum('qkgn,nkd->qkgd', shares.astype(jnp.bfloat16), value_rows, pre...  13.2 us
    reduce_sum x9, other arithmetic, process_probe_group(): row_total = row_total * shrink + jnp.sum(shares, axis=-1)  11.4 us
    dot_general x9, matrix products, process_probe_group(): jnp.einsum('dmvk,hmk->dmvh', probe_entries, matcher_pieces, preferred_ele...  10.8 us
  transfers between devices with their start and end apart: 3, of which 3 were waited for; matrix products, arithmetic and copies ran while one was open for 3% of the time, Pallas kernels for 0%

commit v1 on v0

v1 whole, which is shorter than its diff:
```python
import functools
import math

import jax
import jax.numpy as jnp
from jax import lax
from jax.experimental import pallas as pl
from jax.experimental.pallas import tpu as pltpu
from jax.sharding import Mesh
from jax.sharding import PartitionSpec as P

F32 = jnp.float32
BF16 = jnp.bfloat16
MESH = pl.DeviceIdType.MESH
AXES = ("z", "y", "x", "c")
NZ, NY, NX, NC = 8, 4, 4, 2
NT = NX * NC
D = 2048
HEAD = 64
OWN = 64
TOK = OWN * NT
CTX = 16
COLS = 2 * TOK
GRID_W = 64
EPS = 1e-06
FIRST_SLOTS = 6
LOG2E = math.log2(math.e)


def remote(src, dst, send, recv, device):
    return pltpu.make_async_remote_copy(
        src_ref=src, dst_ref=dst, send_sem=send, recv_sem=recv, device_id=device, device_id_type=MESH
    )


def column(row):
    n = row.shape[1]
    same = lax.broadcasted_iota(jnp.int32, (n, n), 0) == lax.broadcasted_iota(jnp.int32, (n, n), 1)
    return jnp.sum(jnp.where(same, jnp.broadcast_to(row, (n, n)), 0.0), axis=1, keepdims=True)


def kernel(
    latent,
    context,
    condition,
    context_condition,
    norm_gain,
    shift_w,
    scale_w,
    gate_w,
    query_w,
    key_w,
    value_w,
    query_gain,
    key_gain,
    output_w,
    out,
    wmod,
    wcat,
    kw,
    vw,
    wo,
    mod1,
    mod2,
    mod3,
    vecs,
    lat,
    hid,
    tables,
    qraw,
    qhl,
    kv,
    kk,
    vt,
    ctx,
    ckk,
    cvt,
    m_ref,
    o_ref,
    s_ref,
    mx_ref,
    osend,
    lmsend,
    orecv,
    lmrecv,
    asend,
    arecv,
    local_sem,
    mod1_s,
    mod1_r,
    mod2_s,
    mod2_r,
    mod3_s,
    mod3_r,
    lx_s,
    lx_r,
    lf_s,
    lf_r,
    lc_s,
    lc_r,
    q_s,
    q_r,
    kv_s,
    kv_r,
    ctx_s,
    ctx_r,
    o_s,
    o_r,
    lm_s,
    lm_r,
    a_s,
    a_r,
):
    z, y, x, c = (lax.axis_index(a) for a in AXES)
    sp = z * NY + y
    tp = x * NC + c

    def at_z(d):
        return lax.rem(z + d + NZ, NZ)

    def at_y(d):
        return lax.rem(y + d + NY, NY)

    def at_x(d):
        return lax.rem(x + d + NX, NX)

    def tp_peer(d):
        t = lax.rem(tp + d, NT)
        return t, {"x": t // NC, "c": lax.rem(t, NC)}

    odd = lax.rem(sp, 2)
    half = pl.ds(pl.multiple_of(odd * 64, 64), 64)
    other_half = pl.ds(pl.multiple_of((1 - odd) * 64, 64), 64)
    loads = [
        pltpu.make_async_copy(shift_w, wmod.at[half, pl.ds(0, 256)], local_sem.at[0]),
        pltpu.make_async_copy(scale_w, wmod.at[half, pl.ds(256, 256)], local_sem.at[1]),
        pltpu.make_async_copy(gate_w, wmod.at[half, pl.ds(512, 256)], local_sem.at[2]),
        pltpu.make_async_copy(query_w, wcat.at[:, pl.ds(0, 128)], local_sem.at[3]),
        pltpu.make_async_copy(key_w, kw, local_sem.at[4]),
        pltpu.make_async_copy(value_w, vw, local_sem.at[5]),
        pltpu.make_async_copy(output_w, wo, local_sem.at[6]),
        pltpu.make_async_copy(latent, lat.at[tp], local_sem.at[7]),
    ]
    for load in loads:
        load.start()

    barrier = pltpu.get_barrier_semaphore()
    for d in range(1, NZ):
        pl.semaphore_signal(barrier, inc=1, device_id={"z": at_z(d)}, device_id_type=MESH)
    for d in range(1, NY):
        pl.semaphore_signal(barrier, inc=1, device_id={"y": at_y(d)}, device_id_type=MESH)
    for d in range(1, NT):
        pl.semaphore_signal(barrier, inc=1, device_id=tp_peer(d)[1], device_id_type=MESH)

    wmod[other_half, :] = jnp.zeros((64, 768), BF16)
    pair = pl.ds(pl.multiple_of((sp // 2) * 128, 128), 128)
    c0 = jnp.broadcast_to(condition[:, pair], (16, 128))
    c1 = jnp.broadcast_to(context_condition[:, pair], (16, 128))
    line = lax.broadcasted_iota(jnp.int32, (16, 128), 0)
    both = jnp.where(line == 0, c0, jnp.where(line == 1, c1, 0.0))
    activated = (both / (1.0 + jnp.exp(-both))).astype(BF16)
    for load in loads[:3]:
        load.wait()
    part = jnp.dot(activated, wmod[...], preferred_element_type=F32)
    rows = jnp.concatenate(
        [
            part[0:1, 0:256],
            part[0:1, 256:512],
            part[0:1, 512:768],
            part[1:2, 0:256],
            part[1:2, 256:512],
            jnp.zeros((3, 256), F32),
        ],
        axis=0,
    )
    mod1[z] = rows
    loads[7].wait()
    pl.semaphore_wait(barrier, NZ - 1 + NY - 1 + NT - 1)

    top, low = pl.ds(0, 32), pl.ds(32, 32)
    right, left = {"x": at_x(1)}, {"x": at_x(-1)}
    mate = {"c": 1 - c}

    def block_of(d):
        return at_x(d) * NC + c

    def lat_half(d, rows_):
        return lat.at[block_of(d), rows_]

    sends = []

    def go(copy):
        copy.start()
        sends.append(copy)

    go(remote(lat_half(0, top), lat_half(0, top), lx_s.at[0], lx_r.at[0], right))
    go(remote(lat_half(0, low), lat_half(0, low), lx_s.at[1], lx_r.at[1], left))
    for d in range(1, NZ):
        go(remote(mod1.at[z], mod1.at[z], mod1_s.at[d - 1], mod1_r.at[z], {"z": at_z(d)}))
    go(remote(lat_half(0, low), lat_half(0, low), lx_s.at[2], lx_r.at[2], right))
    go(remote(lat_half(0, top), lat_half(0, top), lx_s.at[3], lx_r.at[3], left))
    go(remote(lat.at[tp], lat.at[tp], lc_s.at[0], lc_r.at[0], mate))

    loads[3].wait()
    loads[4].wait()
    loads[5].wait()
    wcat[:, 128:256] = jnp.concatenate([kw[...], vw[...]], axis=1)
    lane = lax.broadcasted_iota(jnp.int32, (16, TOK), 1)
    freq = jnp.exp(
        lax.broadcasted_iota(jnp.int32, (16, TOK), 0).astype(F32) * (-math.log(10000.0) / 16.0)
    )
    row_angle = (lane // GRID_W + sp * (TOK // GRID_W)).astype(F32) * freq
    col_angle = lax.rem(lane, GRID_W).astype(F32) * freq
    tables[0] = jnp.cos(row_angle)
    tables[1] = jnp.sin(row_angle)
    tables[2] = jnp.cos(col_angle)
    tables[3] = jnp.sin(col_angle)
    for r in range(NZ):
        vt[r, 64:80, :] = jnp.ones((16, TOK), BF16)
    cvt[64:80, :] = jnp.ones((16, CTX * NZ), BF16)
    m_ref[...] = jnp.full(m_ref.shape, -1e30, F32)
    o_ref[...] = jnp.zeros(o_ref.shape, F32)

    def arrived(dst, sem):
        remote(dst, dst, lx_s.at[0], sem, mate).wait_recv()

    arrived(lat_half(-1, top), lx_r.at[0])
    go(remote(lat_half(-1, top), lat_half(-1, top), lf_s.at[0], lf_r.at[0], right))
    go(remote(lat_half(-1, top), lat_half(-1, top), lc_s.at[1], lc_r.at[1], mate))
    arrived(lat_half(1, low), lx_r.at[1])
    go(remote(lat_half(1, low), lat_half(1, low), lf_s.at[1], lf_r.at[1], left))
    go(remote(lat_half(1, low), lat_half(1, low), lc_s.at[2], lc_r.at[2], mate))

    for d in range(1, NZ):
        s = at_z(d)
        arrived(mod1.at[s], mod1_r.at[s])
    mod2[y] = jnp.sum(mod1[...], axis=0)
    for d in range(1, NY):
        go(remote(mod2.at[y], mod2.at[y], mod2_s.at[d - 1], mod2_r.at[y], {"y": at_y(d)}))

    arrived(lat_half(-1, low), lx_r.at[2])
    go(remote(lat_half(-1, low), lat_half(-1, low), lc_s.at[3], lc_r.at[3], mate))
    arrived(lat_half(1, top), lx_r.at[3])
    go(remote(lat_half(1, top), lat_half(1, top), lc_s.at[4], lc_r.at[4], mate))

    for d in range(1, NY):
        s = at_y(d)
        arrived(mod2.at[s], mod2_r.at[s])
    mod3[tp] = jnp.sum(mod2[...], axis=0)
    for d in range(1, NT):
        t, device = tp_peer(d)
        go(remote(mod3.at[tp], mod3.at[tp], mod3_s.at[d - 1], mod3_r.at[tp], device))

    arrived(lat_half(2, top), lf_r.at[0])
    go(remote(lat_half(2, top), lat_half(2, top), lc_s.at[5], lc_r.at[5], mate))
    arrived(lat_half(2, low), lf_r.at[1])
    go(remote(lat_half(2, low), lat_half(2, low), lc_s.at[6], lc_r.at[6], mate))

    for d in range(1, NT):
        t, device = tp_peer(d)
        arrived(mod3.at[t], mod3_r.at[t])
    vec = jnp.concatenate([mod3[t] for t in range(NT)], axis=1)
    vecs[0:1] = norm_gain[...] * (1.0 + vec[1:2])
    vecs[1:2] = vec[0:1]
    vecs[2:3] = vec[2:3]
    vecs[3:4] = norm_gain[...] * (1.0 + vec[4:5])
    vecs[4:5] = vec[3:4]

    def modulated(rows_, gain, shift):
        wide = rows_.astype(F32)
        mean = jnp.mean(wide * wide, axis=1, keepdims=True)
        return ((wide * lax.rsqrt(mean + EPS)) * gain + shift).astype(BF16)

    hid[TOK : TOK + CTX, :] = modulated(context[...], vecs[3:4], vecs[4:5])

    def mate_block(d):
        return at_x(d) * NC + 1 - c

    arrived(lat.at[mate_block(0)], lc_r.at[0])
    arrived(lat.at[mate_block(-1), top], lc_r.at[1])
    arrived(lat.at[mate_block(1), low], lc_r.at[2])
    arrived(lat.at[mate_block(-1), low], lc_r.at[3])
    arrived(lat.at[mate_block(1), top], lc_r.at[4])
    arrived(lat.at[mate_block(2), top], lc_r.at[5])
    arrived(lat.at[mate_block(2), low], lc_r.at[6])

    def normalize(i, carry):
        hid[pl.ds(pl.multiple_of(i * 32, 32), 32), :] = modulated(
            lat[i // 2, pl.ds(pl.multiple_of(lax.rem(i, 2) * 32, 32), 32)], vecs[0:1], vecs[1:2]
        )
        return carry

    lax.fori_loop(0, 2 * NT, normalize, 0)

    projected = jnp.dot(hid[...], wcat[...], preferred_element_type=F32)
    turned = projected[0:TOK].T

    def normed(field, gain):
        mean = jnp.mean(field * field, axis=0, keepdims=True)
        return field * lax.rsqrt(mean + EPS) * gain

    def rotated(field):
        cr, sr, cc, sc = tables[0], tables[1], tables[2], tables[3]
        a, b, e, f = field[0:16], field[16:32], field[32:48], field[48:64]
        return jnp.concatenate(
            [a * cr - b * sr, b * cr + a * sr, e * cc - f * sc, f * cc + e * sc], axis=0
        )

    keys = rotated(normed(turned[128:192], column(key_gain[...])))
    packed = jnp.concatenate([keys[:, 0:256], keys[:, 256:512]], axis=0).T
    kv[0, 0:256, :] = packed.astype(BF16)
    values = turned[192:256].astype(BF16)
    for i in range(4):
        kv[0, 256 + 64 * i : 320 + 64 * i, :] = values[:, 128 * i : 128 * (i + 1)]
    cp = projected[TOK : TOK + CTX]
    ck = cp[:, 128:192]
    ck = ck * lax.rsqrt(jnp.mean(ck * ck, axis=1, keepdims=True) + EPS) * key_gain[...]
    ctx[z] = jnp.concatenate([ck, cp[:, 192:256]], axis=1).astype(BF16)

    up, down = {"z": at_z(1)}, {"z": at_z(-1)}
    part_of = (pl.ds(0, 256), pl.ds(256, 256))

    def pass_on(slot, to, chunk, device):
        go(
            remote(
                kv.at[slot, part_of[chunk]],
                kv.at[to, part_of[chunk]],
                kv_s.at[to - 1, chunk],
                kv_r.at[to - 1, chunk],
                device,
            )
        )

    def kv_arrived(slot, chunk):
        dst = kv.at[slot, part_of[chunk]]
        remote(dst, dst, kv_s.at[0, 0], kv_r.at[slot - 1, chunk], up).wait_recv()

    pass_on(0, 1, 0, up)
    pass_on(0, 2, 1, down)
    pass_on(0, 1, 1, up)
    pass_on(0, 2, 0, down)
    for d in range(1, NZ):
        go(remote(ctx.at[z], ctx.at[z], ctx_s.at[d - 1], ctx_r.at[z], {"z": at_z(d)}))

    for h in range(2):
        q = rotated(normed(turned[64 * h : 64 * h + 64], column(query_gain[...])))
        qraw[0, :, TOK * h : TOK * (h + 1)] = q.astype(BF16)
    y_of = (None, {"y": at_y(1)}, {"y": at_y(-1)}, {"y": at_y(2)})
    there = (None, 2, 1, 3)
    for g in range(1, NY):
        go(remote(qraw.at[0], qraw.at[there[g]], q_s.at[g - 1], q_r.at[there[g] - 1], y_of[g]))

    def prepare_queries(g):
        q = qraw[g].astype(F32) * (LOG2E * HEAD ** (-0.5))
        high = q.astype(BF16)
        qhl[g, 0:64, :] = high
        qhl[g, 64:128, :] = (q - high.astype(F32)).astype(BF16)

    def prepare_keys(slot):
        packed_keys = kv[slot, 0:256, :]
        first, second = packed_keys[:, 0:64], packed_keys[:, 64:128]
        kk[slot, 0:256, :] = jnp.concatenate([first, first], axis=1)
        kk[slot, 256:512, :] = jnp.concatenate([second, second], axis=1)
        for i in range(4):
            vt[slot, 0:64, 128 * i : 128 * (i + 1)] = kv[slot, 256 + 64 * i : 320 + 64 * i, :]

    first_tiles = FIRST_SLOTS * NY
    late_slots = NZ - FIRST_SLOTS
    tiles = NZ * NY

    def tile_of(t):
        u = t - first_tiles
        early = t < first_tiles
        slot = jnp.where(early, t // NY, FIRST_SLOTS + lax.rem(u + tiles, late_slots))
        group = jnp.where(early, lax.rem(t, NY), NY - 1 - (u + tiles) // late_slots + tiles // late_slots)
        return slot, group

    def score(t, side):
        slot, group = tile_of(t)
        s = jnp.dot(kk[slot], qhl[group], preferred_element_type=F32)
        s_ref[side] = s
        mx_ref[side] = jnp.max(s, axis=0, keepdims=True)

    def absorb(t, side):
        slot, group = tile_of(t)
        old = m_ref[group]
        new = jnp.maximum(old, mx_ref[side])
        p = jnp.exp2(s_ref[side] - new).astype(BF16)
        m_ref[group] = new
        o_ref[group] = o_ref[group] * jnp.exp2(old - new) + jnp.dot(
            vt[slot], p, preferred_element_type=F32
        )

    def absorb_context(g):
        s = jnp.dot(ckk[...], qhl[g], preferred_element_type=F32) + math.log2(TOK / (2.0 * CTX))
        old = m_ref[g]
        new = jnp.maximum(old, jnp.max(s, axis=0, keepdims=True))
        p = jnp.exp2(s - new).astype(BF16)
        m_ref[g] = new
        o_ref[g] = o_ref[g] * jnp.exp2(old - new) + jnp.dot(
            cvt[...], p, preferred_element_type=F32
        )

    def send_out(g):
        osend[g - 1] = o_ref[g, 0:64, :].astype(BF16)
        lmsend[g - 1, 0:1, :] = o_ref[g, 64:65, :]
        lmsend[g - 1, 1:2, :] = m_ref[g]
        to = there[g] - 1
        remote(osend.at[g - 1], orecv.at[to], o_s.at[g - 1], o_r.at[to], y_of[g]).start()
        remote(lmsend.at[g - 1], lmrecv.at[to], lm_s.at[g - 1], lm_r.at[to], y_of[g]).start()

    prepare_keys(0)
    prepare_queries(0)
    score(0, 0)
    for slot, chunk in ((1, 0), (2, 1), (1, 1), (2, 0)):
        kv_arrived(slot, chunk)
        pass_on(slot, slot + 2, chunk, up if slot == 1 else down)
    prepare_keys(1)
    prepare_keys(2)
    for g in (1, 2):
        dst = qraw.at[g]
        remote(dst, dst, q_s.at[0], q_r.at[g - 1], up).wait_recv()
        prepare_queries(g)

    later = []

    def body(j, carry):
        @pl.when(j == 1)
        def _():
            dst = qraw.at[3]
            remote(dst, dst, q_s.at[0], q_r.at[2], up).wait_recv()
            prepare_queries(3)

        @pl.when(j == 4)
        def _():
            for slot, chunk in ((3, 0), (4, 1)):
                kv_arrived(slot, chunk)
                fwd(slot, chunk)

        @pl.when(j == 5)
        def _():
            for slot, chunk in ((3, 1), (4, 0)):
                kv_arrived(slot, chunk)
                fwd(slot, chunk)
            prepare_keys(3)
            prepare_keys(4)

        @pl.when(j == 8)
        def _():
            for slot, chunk in ((5, 0), (6, 1)):
                kv_arrived(slot, chunk)
                fwd(slot, chunk)

        @pl.when(j == 9)
        def _():
            for slot, chunk in ((5, 1), (6, 0)):
                kv_arrived(slot, chunk)
            prepare_keys(5)
            prepare_keys(6)

        @pl.when(j == 12)
        def _():
            kv_arrived(7, 0)
            kv_arrived(7, 1)
            prepare_keys(7)
            for d in range(1, NZ):
                s = at_z(d)
                arrived(ctx.at[s], ctx_r.at[s])
            every = ctx[...].reshape(NZ * CTX, 128)
            ckk[...] = jnp.concatenate([every[:, 0:64], every[:, 0:64]], axis=1)
            cvt[0:64, :] = every.astype(F32).T[64:128].astype(BF16)
            for g in range(NY):
                absorb_context(g)

        for k, g in ((13, 3), (14, 2), (15, 1)):
            pl.when(j == k)(functools.partial(send_out, g))

        for u in range(2):
            t = 2 * j + u
            score(jnp.minimum(t + 1, tiles - 1), (u + 1) % 2)
            absorb(t, u % 2)
        return carry

    def fwd(slot, chunk):
        to = min(slot + 2, 7)
        remote(
            kv.at[slot, part_of[chunk]],
            kv.at[to, part_of[chunk]],
            kv_s.at[to - 1, chunk],
            kv_r.at[to - 1, chunk],
            up if slot % 2 == 1 else down,
        ).start()
        later.append((slot, to, chunk))

    lax.fori_loop(0, tiles // 2, body, 0)

    top_m = m_ref[0]
    for i in range(NY - 1):
        dst = lmrecv.at[i]
        remote(dst, dst, lm_s.at[0], lm_r.at[i], up).wait_recv()
        top_m = jnp.maximum(top_m, lmrecv[i, 1:2, :])
    weight = jnp.exp2(m_ref[0] - top_m)
    total = o_ref[0, 64:65, :] * weight
    mixed = o_ref[0, 0:64, :] * weight
    for i in (2, 1, 0):
        dst = orecv.at[i]
        remote(dst, dst, o_s.at[0], o_r.at[i], up).wait_recv()
        weight = jnp.exp2(lmrecv[i, 1:2, :] - top_m)
        total = total + lmrecv[i, 0:1, :] * weight
        mixed = mixed + orecv[i].astype(F32) * weight
    mixed = mixed / total
    attended = jnp.concatenate([mixed[:, 0:TOK], mixed[:, TOK:COLS]], axis=0).T.astype(BF16)
    for t in range(NT):
        asend[t] = attended[OWN * t : OWN * (t + 1)]
    arecv[tp] = asend[tp]
    for d in range(1, NT):
        t, device = tp_peer(d)
        go(remote(asend.at[t], arecv.at[tp], a_s.at[d - 1], a_r.at[tp], device))
    loads[6].wait()
    for d in range(1, NT):
        t, device = tp_peer(d)
        arrived(arecv.at[t], a_r.at[t])
    heads = jnp.concatenate([arecv[t] for t in range(NT)], axis=1)
    for i in range(4):
        cols = slice(512 * i, 512 * (i + 1))
        branch = jnp.dot(heads, wo[:, cols], preferred_element_type=F32)
        out[:, cols] = (
            lat[tp, :, cols].astype(F32) + vecs[2:3, cols] * branch
        ).astype(BF16)

    for copy in sends:
        copy.wait_send()
    for slot, to, chunk in later:
        remote(
            kv.at[slot, part_of[chunk]],
            kv.at[to, part_of[chunk]],
            kv_s.at[to - 1, chunk],
            kv_r.at[to - 1, chunk],
            up,
        ).wait_send()
    for g in range(1, NY):
        remote(osend.at[g - 1], orecv.at[g - 1], o_s.at[g - 1], o_r.at[g - 1], up).wait_send()
        remote(lmsend.at[g - 1], lmrecv.at[g - 1], lm_s.at[g - 1], lm_r.at[g - 1], up).wait_send()


def on_device(
    latent,
    context,
    condition,
    context_condition,
    norm_gain,
    shift_weight,
    scale_weight,
    gate_weight,
    query_weight,
    key_weight,
    value_weight,
    query_gain,
    key_gain,
    output_weight,
):
    vmem, hbm = pl.BlockSpec(memory_space=pltpu.VMEM), pl.BlockSpec(memory_space=pl.ANY)
    dma, V = pltpu.SemaphoreType.DMA, pltpu.VMEM
    return pl.pallas_call(
        kernel,
        out_shape=jax.ShapeDtypeStruct((OWN, D), BF16),
        in_specs=[hbm, vmem, vmem, vmem, vmem] + [hbm] * 6 + [vmem, vmem, hbm],
        out_specs=vmem,
        scratch_shapes=[
            V((128, 768), BF16),
            V((D, 256), BF16),
            V((D, 64), BF16),
            V((D, 64), BF16),
            V((1024, D), BF16),
            V((NZ, 8, 256), F32),
            V((NY, 8, 256), F32),
            V((NT, 8, 256), F32),
            V((8, D), F32),
            V((NT, OWN, D), BF16),
            V((TOK + CTX, D), BF16),
            V((4, 16, TOK), F32),
            V((NY, HEAD, COLS), BF16),
            V((NY, 2 * HEAD, COLS), BF16),
            V((NZ, 512, 128), BF16),
            V((NZ, TOK, 128), BF16),
            V((NZ, 80, TOK), BF16),
            V((NZ, CTX, 128), BF16),
            V((NZ * CTX, 128), BF16),
            V((80, NZ * CTX), BF16),
            V((NY, 1, COLS), F32),
            V((NY, 80, COLS), F32),
            V((2, TOK, COLS), F32),
            V((2, 1, COLS), F32),
            V((NY - 1, HEAD, COLS), BF16),
            V((NY - 1, 8, COLS), F32),
            V((NY - 1, HEAD, COLS), BF16),
            V((NY - 1, 8, COLS), F32),
            V((NT, OWN, 128), BF16),
            V((NT, OWN, 128), BF16),
            dma((8,)),
            dma((NZ - 1,)),
            dma((NZ,)),
            dma((NY - 1,)),
            dma((NY,)),
            dma((NT - 1,)),
            dma((NT,)),
            dma((4,)),
            dma((4,)),
            dma((2,)),
            dma((2,)),
            dma((7,)),
            dma((7,)),
            dma((NY - 1,)),
            dma((NY - 1,)),
            dma((NZ - 1, 2)),
            dma((NZ - 1, 2)),
            dma((NZ - 1,)),
            dma((NZ,)),
            dma((NY - 1,)),
            dma((NY - 1,)),
            dma((NY - 1,)),
            dma((NY - 1,)),
            dma((NT - 1,)),
            dma((NT,)),
        ],
        compiler_params=pltpu.CompilerParams(
            collective_id=0, has_side_effects=True, vmem_limit_bytes=60 * 2**20
        ),
    )(
        latent,
        context,
        condition.reshape(1, D),
        context_condition.reshape(1, D),
        norm_gain.reshape(1, D),
        shift_weight,
        scale_weight,
        gate_weight,
        query_weight,
        key_weight,
        value_weight,
        query_gain.reshape(1, HEAD),
        key_gain.reshape(1, HEAD),
        output_weight,
    )


def solution(mesh):
    split = Mesh(mesh.devices.reshape(NZ, NY, NX, NC), AXES)
    seq, tp, everything = ("z", "y"), ("x", "c"), AXES
    return jax.shard_map(
        on_device,
        mesh=split,
        in_specs=(
            P(everything, None),
            P(seq, None),
            P(),
            P(),
            P(),
            P(seq, tp),
            P(seq, tp),
            P(seq, tp),
            P(None, tp),
            P(None, tp),
            P(None, tp),
            P(),
            P(),
            P(),
        ),
        out_specs=P(everything, None),
        check_vma=False,
    )
```

time: 219 us -> 74.5 us (0.34)
  Pallas kernels: 0 us -> 68.7 us
  blocking collectives: 67.3 us -> 0 us
  waiting for transfers between devices: 52.4 us -> 0 us
  matrix products: 33.1 us -> 0 us
  other arithmetic: 16.7 us -> 0 us
  starting transfers between devices: 16 us -> 0 us
  between operations: 13.7 us -> 0.01 us
  local copies, waits for them, and re-layouts: 18.5 us -> 5.59 us
    pallas_call x0 -> x1, Pallas kernels: none -> 68.7 us  [on_device(): pl.pallas_call(kernel, out_shape=jax.ShapeDtypeStruct((OWN, D), BF16), in...]
    all_gather x4 -> x0, blocking collectives: 57.2 us -> none  [the longest x3 41.6 us: whole_of(): result = lax.all_gather(result, axes[number], axis=dim, tiled=True)]
    dot_general x24 -> x0, matrix products: 33.1 us -> none  [the longest x9 13.2 us: process_probe_group(): jnp.einsum('qkgn,nkd->qkgd', shares.astype(jnp.bfloat16), value_rows, pre...]
    all_to_all x2 -> x0, waiting for transfers between devices: 33 us -> none  [from_everyone(): lax.all_to_all(jnp.broadcast_to(array[None], (devices, *array.shape)), ax...]
    all_gather x1 -> x0, waiting for transfers between devices: 19.4 us -> none  [whole_of(): result = lax.all_gather(result, axes[number], axis=dim, tiled=True)]
    all_to_all x2 -> x0, starting transfers between devices: 16 us -> none  [from_everyone(): lax.all_to_all(jnp.broadcast_to(array[None], (devices, *array.shape)), ax...]
    reduce_sum x15 -> x0, other arithmetic: 13 us -> none  [the longest x9 11.4 us: process_probe_group(): row_total = row_total * shrink + jnp.sum(shares, axis=-1)]
    all_to_all x1 -> x0, blocking collectives: 10.1 us -> none  [on_device(): lax.all_to_all(attended, 'tp', split_axis=0, concat_axis=1, tiled=True)]
  transfers between devices with their start and end apart: 3 -> 0, of which waited for: 3 -> 0; matrix products, arithmetic and copies ran while one was open for 3% -> 0% of each run, Pallas kernels for 0% -> 0%
where the time goes in v1:
time: 74.5 us; the launch traced here: 74.3 us
  Pallas kernels  68.7 us (92%)
  local copies, waits for them, and re-layouts  5.59 us (8%)
    pallas_call x1, Pallas kernels, on_device(): pl.pallas_call(kernel, out_shape=jax.ShapeDtypeStruct((OWN, D), BF16), in...  68.7 us
    unnamed x3, local copies, waits for them, and re-layouts  5.59 us

profile of v1, /device:TPU:1, one launch (start us, length us, event | category | flops | bytes accessed | tf_op | source)
XLA Modules:
  0.0 74.3 jit_solution(8301605566238354641)
XLA Ops:
  0.0 1.9 %copy.15.key_w = bf16[2048,64]{1,0:T(8,128)(2,1)} copy(bf16[2048,64]{0,1:T(8,128)(2,1)} %param.23) | data formatting | bytes 524288 | tf_op args[9]
  1.9 2.0 %copy.16.value_w = bf16[2048,64]{1,0:T(8,128)(2,1)} copy(bf16[2048,64]{0,1:T(8,128)(2,1)} %param.24) | data formatting | bytes 524288 | tf_op args[10]
  3.9 68.7 %shard_map.136 = bf16[64,2048]{1,0:T(8,128)(2,1)} custom-call(bf16[64,2048]{1,0:T(8,128)(2,1)} %latent.1, bf16[16,2048]{1,0:T(8,128)(2,1)} %context.1, f32[1,2048]{1,0:T(1,128)} %bitcast.5, f32[1,2048]{1,0:T(1,128)} %bitcast.6, f32[1,2048]{1,0:T(1,128)} %bitcast.7, bf16[64,256]{1,0:T(8,128)(2,1)} %shift_w.1, bf16[64,256]{1,0:T(8,128)(2,1)} %scale_w.1, ...), custom_call_target="tpu_custom_call" | custom-call | tf_op jit(solution)/shard_map/pallas_call | solution.py:564
  72.6 1.7 %copy.18 = bf16[64,2048]{1,0:T(8,128)(2,1)} copy(bf16[64,2048]{1,0:T(8,128)(2,1)} %shard_map.136) | data formatting | bytes 524288

commit v2 on v1

v2 whole, which is shorter than its diff:
```python
import functools
import math

import jax
import jax.numpy as jnp
from jax import lax
from jax.experimental import pallas as pl
from jax.experimental.pallas import tpu as pltpu
from jax.sharding import Mesh
from jax.sharding import PartitionSpec as P

F32 = jnp.float32
BF16 = jnp.bfloat16
MESH = pl.DeviceIdType.MESH
AXES = ("z", "y", "x", "c")
NZ, NY, NX, NC = 8, 4, 4, 2
NT = NX * NC
D = 2048
HEAD = 64
OWN = 64
TOK = OWN * NT
QUARTER = TOK // NX
ORDER = (0, -1, 1, 2)
CTX = 16
COLS = 2 * TOK
GRID_W = 64
EPS = 1e-06
LOG2E = math.log2(math.e)


def remote(src, dst, send, recv, device):
    return pltpu.make_async_remote_copy(
        src_ref=src, dst_ref=dst, send_sem=send, recv_sem=recv, device_id=device, device_id_type=MESH
    )


def column(row):
    n = row.shape[1]
    same = lax.broadcasted_iota(jnp.int32, (n, n), 0) == lax.broadcasted_iota(jnp.int32, (n, n), 1)
    return jnp.sum(jnp.where(same, jnp.broadcast_to(row, (n, n)), 0.0), axis=1, keepdims=True)


def kernel(
    latent,
    context_in,
    condition_in,
    context_condition_in,
    norm_gain_in,
    shift_w,
    scale_w,
    gate_w,
    query_w,
    key_w,
    value_w,
    query_gain_in,
    key_gain_in,
    output_w,
    out,
    context,
    condition,
    context_condition,
    norm_gain,
    query_gain,
    key_gain,
    result,
    wmod,
    wcat,
    kvw,
    wo,
    mod1,
    mod2,
    mod3,
    vecs,
    lat,
    hid,
    tables,
    qraw,
    qhl,
    kv,
    kk,
    vt,
    ctx,
    ckk,
    cvt,
    m_ref,
    o_ref,
    s_ref,
    mx_ref,
    osend,
    lmsend,
    orecv,
    lmrecv,
    asend,
    arecv,
    local_sem,
    out_sem,
    mod1_s,
    mod1_r,
    mod2_s,
    mod2_r,
    mod3_s,
    mod3_r,
    lat_s,
    lx_r,
    lf_r,
    lc_r,
    q_s,
    q_r,
    kv_s,
    kv_r,
    ctx_s,
    ctx_r,
    o_s,
    o_r,
    lm_s,
    lm_r,
    a_s,
    a_r,
):
    z, y, x, c = (lax.axis_index(a) for a in AXES)
    sp = z * NY + y
    tp = x * NC + c

    def at_z(d):
        return lax.rem(z + d + NZ, NZ)

    def at_y(d):
        return lax.rem(y + d + NY, NY)

    def at_x(d):
        return lax.rem(x + d + NX, NX)

    def tp_peer(d):
        t = lax.rem(tp + d, NT)
        return t, {"x": t // NC, "c": lax.rem(t, NC)}

    odd = lax.rem(sp, 2)
    half = pl.ds(pl.multiple_of(odd * 64, 64), 64)
    other_half = pl.ds(pl.multiple_of((1 - odd) * 64, 64), 64)
    loads = [
        pltpu.make_async_copy(shift_w, wmod.at[half, pl.ds(0, 256)], local_sem.at[0]),
        pltpu.make_async_copy(scale_w, wmod.at[half, pl.ds(256, 256)], local_sem.at[1]),
        pltpu.make_async_copy(gate_w, wmod.at[half, pl.ds(512, 256)], local_sem.at[2]),
        pltpu.make_async_copy(query_w, wcat.at[:, pl.ds(0, 128)], local_sem.at[3]),
        pltpu.make_async_copy(key_w, kvw.at[pl.ds(0, 64)], local_sem.at[4]),
        pltpu.make_async_copy(value_w, kvw.at[pl.ds(64, 64)], local_sem.at[5]),
        pltpu.make_async_copy(output_w, wo, local_sem.at[6]),
        pltpu.make_async_copy(latent, lat.at[tp], local_sem.at[7]),
        pltpu.make_async_copy(condition_in, condition, local_sem.at[8]),
        pltpu.make_async_copy(context_condition_in, context_condition, local_sem.at[9]),
        pltpu.make_async_copy(context_in, context, local_sem.at[10]),
        pltpu.make_async_copy(norm_gain_in, norm_gain, local_sem.at[11]),
        pltpu.make_async_copy(query_gain_in, query_gain, local_sem.at[12]),
        pltpu.make_async_copy(key_gain_in, key_gain, local_sem.at[13]),
    ]
    for i in (8, 9, 0, 1, 2, 7, 3, 4, 5, 10, 11, 12, 13, 6):
        loads[i].start()

    barrier = pltpu.get_barrier_semaphore()
    for d in range(1, NZ):
        pl.semaphore_signal(barrier, inc=1, device_id={"z": at_z(d)}, device_id_type=MESH)
    for d in range(1, NY):
        pl.semaphore_signal(barrier, inc=1, device_id={"y": at_y(d)}, device_id_type=MESH)
    for d in range(1, NT):
        pl.semaphore_signal(barrier, inc=1, device_id=tp_peer(d)[1], device_id_type=MESH)

    wmod[other_half, :] = jnp.zeros((64, 768), BF16)
    pair = pl.ds(pl.multiple_of((sp // 2) * 128, 128), 128)
    loads[8].wait()
    loads[9].wait()
    c0 = jnp.broadcast_to(condition[:, pair], (16, 128))
    c1 = jnp.broadcast_to(context_condition[:, pair], (16, 128))
    line = lax.broadcasted_iota(jnp.int32, (16, 128), 0)
    both = jnp.where(line == 0, c0, jnp.where(line == 1, c1, 0.0))
    activated = (both / (1.0 + jnp.exp(-both))).astype(BF16)
    for load in loads[:3]:
        load.wait()
    part = jnp.dot(activated, wmod[...], preferred_element_type=F32)
    rows = jnp.concatenate(
        [
            part[0:1, 0:256],
            part[0:1, 256:512],
            part[0:1, 512:768],
            part[1:2, 0:256],
            part[1:2, 256:512],
            jnp.zeros((3, 256), F32),
        ],
        axis=0,
    )
    mod1[z] = rows
    loads[7].wait()
    pl.semaphore_wait(barrier, NZ - 1 + NY - 1 + NT - 1)

    top, low = pl.ds(0, 32), pl.ds(32, 32)
    right, left = {"x": at_x(1)}, {"x": at_x(-1)}
    mate = {"c": 1 - c}

    def block_of(d):
        return at_x(d) * NC + c

    def lat_half(d, rows_):
        return lat.at[block_of(d), rows_]

    def go(copy):
        copy.start()

    go(remote(lat_half(0, top), lat_half(0, top), lat_s, lx_r.at[0], right))
    go(remote(lat_half(0, low), lat_half(0, low), lat_s, lx_r.at[1], left))
    for d in range(1, NZ):
        go(remote(mod1.at[z], mod1.at[z], mod1_s, mod1_r, {"z": at_z(d)}))
    go(remote(lat_half(0, low), lat_half(0, low), lat_s, lx_r.at[2], right))
    go(remote(lat_half(0, top), lat_half(0, top), lat_s, lx_r.at[3], left))
    go(remote(lat.at[tp], lat.at[tp], lat_s, lc_r.at[0], mate))

    loads[3].wait()
    loads[4].wait()
    loads[5].wait()
    wcat[:, 128:256] = kvw[...].T
    for load in loads[10:]:
        load.wait()
    lane = lax.broadcasted_iota(jnp.int32, (16, TOK), 1)
    freq = jnp.exp(
        lax.broadcasted_iota(jnp.int32, (16, TOK), 0).astype(F32) * (-math.log(10000.0) / 16.0)
    )
    row_angle = (lane // GRID_W + sp * (TOK // GRID_W)).astype(F32) * freq
    col_angle = lax.rem(lane, GRID_W).astype(F32) * freq
    tables[0] = jnp.cos(row_angle)
    tables[1] = jnp.sin(row_angle)
    tables[2] = jnp.cos(col_angle)
    tables[3] = jnp.sin(col_angle)
    for r in range(NZ):
        vt[r, 64:80, :] = jnp.ones((16, TOK), BF16)
    key_column, query_column = column(key_gain[...]), column(query_gain[...])
    cvt[64:80, :] = jnp.ones((16, CTX * NZ), BF16)
    m_ref[...] = jnp.full(m_ref.shape, -1e30, F32)
    o_ref[...] = jnp.zeros(o_ref.shape, F32)

    def arrived(dst, sem):
        remote(dst, dst, lat_s, sem, mate).wait_recv()

    arrived(mod1.at[pl.ds(0, NZ - 1)], mod1_r)
    mod2[y] = jnp.sum(mod1[...], axis=0)
    for d in range(1, NY):
        go(remote(mod2.at[y], mod2.at[y], mod2_s, mod2_r, {"y": at_y(d)}))

    piece = [pl.ds(16 * i, 16) for i in range(4)]

    def relay(d, i, device):
        go(remote(lat_half(d, piece[i]), lat_half(d, piece[i]), lat_s, lf_r.at[i], device))

    arrived(lat_half(-1, top), lx_r.at[0])
    relay(-1, 0, right)
    go(remote(lat_half(-1, top), lat_half(-1, top), lat_s, lc_r.at[1], mate))
    arrived(lat_half(1, low), lx_r.at[1])
    relay(1, 2, left)
    go(remote(lat_half(1, low), lat_half(1, low), lat_s, lc_r.at[2], mate))

    arrived(mod2.at[pl.ds(0, NY - 1)], mod2_r)
    mod3[tp] = jnp.sum(mod2[...], axis=0)
    for d in range(1, NT):
        t, device = tp_peer(d)
        go(remote(mod3.at[tp], mod3.at[tp], mod3_s, mod3_r, device))
    relay(-1, 1, right)
    relay(1, 3, left)

    arrived(lat_half(-1, low), lx_r.at[2])
    go(remote(lat_half(-1, low), lat_half(-1, low), lat_s, lc_r.at[3], mate))
    arrived(lat_half(1, top), lx_r.at[3])
    go(remote(lat_half(1, top), lat_half(1, top), lat_s, lc_r.at[4], mate))

    arrived(mod3.at[pl.ds(0, NT - 1)], mod3_r)
    vec = jnp.concatenate([mod3[t] for t in range(NT)], axis=1)
    vecs[0:1] = norm_gain[...] * (1.0 + vec[1:2])
    vecs[1:2] = vec[0:1]
    vecs[2:3] = vec[2:3]
    vecs[3:4] = norm_gain[...] * (1.0 + vec[4:5])
    vecs[4:5] = vec[3:4]

    def modulated(rows_, gain, shift):
        wide = rows_.astype(F32)
        mean = jnp.mean(wide * wide, axis=1, keepdims=True)
        return ((wide * lax.rsqrt(mean + EPS)) * gain + shift).astype(BF16)

    hid[QUARTER:, :] = modulated(context[...], vecs[3:4], vecs[4:5])

    def normed(field, gain):
        mean = jnp.mean(field * field, axis=0, keepdims=True)
        return field * lax.rsqrt(mean + EPS) * gain

    up, down = {"z": at_z(1)}, {"z": at_z(-1)}
    y_of = (None, {"y": at_y(1)}, {"y": at_y(-1)}, {"y": at_y(2)})
    there = (None, 2, 1, 3)

    def part_of(i):
        return pl.ds(pl.multiple_of(at_x(ORDER[i]) * QUARTER, QUARTER), QUARTER)

    def kv_copy(slot, to, i):
        return remote(
            kv.at[slot, part_of(i)],
            kv.at[to, part_of(i)],
            kv_s,
            kv_r.at[to - 1, i],
            down if to in (2, 4, 6) or slot == 6 else up,
        )

    def kv_arrived(slot, i):
        dst = kv.at[slot, part_of(i)]
        remote(dst, dst, kv_s, kv_r.at[slot - 1, i], up).wait_recv()

    def process(i):
        xb = at_x(ORDER[i])

        def normalize(k, carry):
            hid[pl.ds(pl.multiple_of(k * 32, 32), 32), :] = modulated(
                lat[xb * NC + k // 2, pl.ds(pl.multiple_of(lax.rem(k, 2) * 32, 32), 32)],
                vecs[0:1],
                vecs[1:2],
            )
            return carry

        lax.fori_loop(0, QUARTER // 32, normalize, 0)
        many = QUARTER + CTX if i == 0 else QUARTER
        projected = jnp.dot(hid[0:many], wcat[...], preferred_element_type=F32)
        turned = projected[0:QUARTER].T
        lanes = pl.ds(pl.multiple_of(xb * QUARTER, QUARTER), QUARTER)
        cr, sr, cc, sc = (tables[k, :, lanes] for k in range(4))

        def rotated(field):
            a, b, e, f = field[0:16], field[16:32], field[32:48], field[48:64]
            return jnp.concatenate(
                [a * cr - b * sr, b * cr + a * sr, e * cc - f * sc, f * cc + e * sc], axis=0
            )

        keys = rotated(normed(turned[128:192], key_column))
        packed = jnp.concatenate([keys[:, 0:64], keys[:, 64:128]], axis=0).T
        first = pl.multiple_of(xb * QUARTER, QUARTER)
        kv[0, pl.ds(first, 64), :] = packed.astype(BF16)
        kv[0, pl.ds(first + 64, 64), :] = turned[192:256].astype(BF16)
        go(kv_copy(0, 1, i))
        go(kv_copy(0, 2, i))
        for h in range(2):
            q = rotated(normed(turned[64 * h : 64 * h + 64], query_column))
            qraw[0, xb, :, QUARTER * h : QUARTER * (h + 1)] = q.astype(BF16)
        for g in range(1, NY):
            go(
                remote(
                    qraw.at[0, xb],
                    qraw.at[there[g], xb],
                    q_s,
                    q_r.at[there[g] - 1],
                    y_of[g],
                )
            )
        if i == 0:
            cp = projected[QUARTER : QUARTER + CTX]
            ck = cp[:, 128:192]
            ck = ck * lax.rsqrt(jnp.mean(ck * ck, axis=1, keepdims=True) + EPS) * key_gain[...]
            ctx[z] = jnp.concatenate([ck, cp[:, 192:256]], axis=1).astype(BF16)
            for d in range(1, NZ):
                go(remote(ctx.at[z], ctx.at[z], ctx_s, ctx_r, {"z": at_z(d)}))

    def mate_block(d):
        return at_x(d) * NC + 1 - c

    arrived(lat.at[mate_block(0)], lc_r.at[0])
    process(0)

    arrived(lat_half(2, piece[0]), lf_r.at[0])
    arrived(lat_half(2, piece[1]), lf_r.at[1])
    go(remote(lat_half(2, top), lat_half(2, top), lat_s, lc_r.at[5], mate))
    arrived(lat_half(2, piece[2]), lf_r.at[2])
    arrived(lat_half(2, piece[3]), lf_r.at[3])
    go(remote(lat_half(2, low), lat_half(2, low), lat_s, lc_r.at[6], mate))

    arrived(lat.at[mate_block(-1), top], lc_r.at[1])
    arrived(lat.at[mate_block(-1), low], lc_r.at[3])
    process(1)

    arrived(lat.at[mate_block(1), low], lc_r.at[2])
    arrived(lat.at[mate_block(1), top], lc_r.at[4])
    process(2)

    arrived(lat.at[mate_block(2), top], lc_r.at[5])
    arrived(lat.at[mate_block(2), low], lc_r.at[6])

    process(3)

    def prepare_queries(g):
        for k in range(NX):
            q = qraw[g, k].astype(F32) * (LOG2E * HEAD ** (-0.5))
            high = q.astype(BF16)
            cols = slice(2 * QUARTER * k, 2 * QUARTER * (k + 1))
            qhl[g, 0:64, cols] = high
            qhl[g, 64:128, cols] = (q - high.astype(F32)).astype(BF16)

    def prepare_keys(slot):
        for k in range(NX):
            first = QUARTER * k
            packed_keys = kv[slot, first : first + 64, :]
            low_lanes, high_lanes = packed_keys[:, 0:64], packed_keys[:, 64:128]
            kk[slot, first : first + 64, :] = jnp.concatenate([low_lanes, low_lanes], axis=1)
            kk[slot, first + 64 : first + 128, :] = jnp.concatenate([high_lanes, high_lanes], axis=1)
            vt[slot, 0:64, first : first + QUARTER] = kv[slot, first + 64 : first + QUARTER, :]

    tiles = NZ * NY

    def pick(cases, default):
        for test, value in reversed(cases):
            default = jnp.where(test, value, default)
        return default

    def tile_of(t):
        w, v = t - 1 + 6, t - 19 + 20
        slot = pick(
            [(t < 1, 0), (t < 5, w // 2 - 3), (t < 7, t - 5), (t < 19, w // 3 - 2), (t < 25, 6 + lax.rem(v, 2))],
            t - 24,
        )
        group = pick(
            [(t < 1, 0), (t < 5, 1 + lax.rem(w, 2)), (t < 7, 3), (t < 19, 1 + lax.rem(w, 3)), (t < 25, 13 - v // 2)],
            0,
        )
        return slot, group

    strips = [pl.ds(256 * k, 256) for k in range(COLS // 256)]

    def score_strip(tile, side, cols):
        slot, group = tile
        s = jnp.dot(kk[slot], qhl[group, :, cols], preferred_element_type=F32)
        s_ref[side, :, cols] = s
        mx_ref[side, :, cols] = jnp.max(s, axis=0, keepdims=True)

    def absorb_strip(tile, side, cols):
        slot, group = tile
        old = m_ref[group, :, cols]
        new = jnp.maximum(old, mx_ref[side, :, cols])
        p = jnp.exp2(s_ref[side, :, cols] - new).astype(BF16)
        m_ref[group, :, cols] = new
        o_ref[group, :, cols] = o_ref[group, :, cols] * jnp.exp2(old - new) + jnp.dot(
            vt[slot], p, preferred_element_type=F32
        )

    def score(t, side):
        for cols in strips:
            score_strip(tile_of(t), side, cols)

    def absorb(t, side):
        for cols in strips:
            absorb_strip(tile_of(t), side, cols)

    def absorb_context(g):
        s = jnp.dot(ckk[...], qhl[g], preferred_element_type=F32) + math.log2(TOK / (2.0 * CTX))
        old = m_ref[g]
        new = jnp.maximum(old, jnp.max(s, axis=0, keepdims=True))
        p = jnp.exp2(s - new).astype(BF16)
        m_ref[g] = new
        o_ref[g] = o_ref[g] * jnp.exp2(old - new) + jnp.dot(
            cvt[...], p, preferred_element_type=F32
        )

    def send_out(g):
        osend[g - 1] = o_ref[g, 0:64, :].astype(BF16)
        for i in range(4):
            lmsend[g - 1, i : i + 1, :] = o_ref[g, 64:65, 256 * i : 256 * (i + 1)]
            lmsend[g - 1, 4 + i : 5 + i, :] = m_ref[g, :, 256 * i : 256 * (i + 1)]
        to = there[g] - 1
        remote(osend.at[g - 1], orecv.at[to], o_s, o_r, y_of[g]).start()
        remote(lmsend.at[g - 1], lmrecv.at[to], lm_s, lm_r, y_of[g]).start()

    def pass_on(i):
        for slot in (1, 2):
            kv_arrived(slot, i)
            go(kv_copy(slot, slot + 2, i))

    prepare_keys(0)
    prepare_queries(0)
    pass_on(0)
    score(0, 0)
    absorb(0, 0)

    pass_on(1)
    pass_on(2)
    pass_on(3)
    prepare_keys(1)
    prepare_keys(2)

    def queries_arrived(g):
        remote(qraw.at[g], qraw.at[g], q_s, q_r.at[g - 1], up).wait_recv()
        prepare_queries(g)

    queries_arrived(1)
    queries_arrived(2)
    score(1, 1)

    def body(j, carry):
        @pl.when(j == 1)
        def _():
            queries_arrived(3)

        @pl.when(j == 1)
        def _():
            for slot in (3, 4):
                kv_arrived(slot, 0)
                fwd(slot, 0)

        @pl.when(j == 2)
        def _():
            for i in (1, 2):
                for slot in (3, 4):
                    kv_arrived(slot, i)
                    fwd(slot, i)

        @pl.when(j == 3)
        def _():
            for slot in (3, 4):
                kv_arrived(slot, 3)
                fwd(slot, 3)
            prepare_keys(3)
            prepare_keys(4)

        @pl.when(j == 5)
        def _():
            for i in (0, 1):
                kv_arrived(5, i)
                fwd(5, i)
                kv_arrived(6, i)

        @pl.when(j == 6)
        def _():
            for i in (2, 3):
                kv_arrived(6, i)
                fwd(6, i)
                kv_arrived(5, i)
            prepare_keys(5)
            prepare_keys(6)

        @pl.when(j == 9)
        def _():
            for i in range(NX):
                kv_arrived(7, i)
            prepare_keys(7)
            arrived(ctx.at[pl.ds(0, NZ - 1)], ctx_r)
            every = ctx[...].reshape(NZ * CTX, 128)
            ckk[...] = jnp.concatenate([every[:, 0:64], every[:, 0:64]], axis=1)
            cvt[0:64, :] = every.astype(F32).T[64:128].astype(BF16)
            for g in range(NY):
                absorb_context(g)

        for k, g in ((10, 3), (11, 2), (12, 1)):
            pl.when(j == k)(functools.partial(send_out, g))

        now = tile_of(2 * j + 1)
        for u in range(2):
            t = 2 * j + 1 + u
            side = (u + 1) % 2
            following = tile_of(t + 1)
            for cols in strips:
                score_strip(following, 1 - side, cols)
                absorb_strip(now, side, cols)
            now = following
        return carry

    def fwd(slot, i):
        copy = kv_copy(slot, min(slot + 2, 7), i)
        copy.start()

    lax.fori_loop(0, tiles // 2 - 1, body, 0)
    absorb(tiles - 1, 1)

    def unpacked(i, first):
        return jnp.concatenate([lmrecv[i, first + k : first + k + 1, :] for k in range(4)], axis=1)

    top_m = m_ref[0]
    remote(lmrecv, lmrecv, lm_s, lm_r, up).wait_recv()
    for i in range(NY - 1):
        top_m = jnp.maximum(top_m, unpacked(i, 4))
    weight = jnp.exp2(m_ref[0] - top_m)
    total = o_ref[0, 64:65, :] * weight
    mixed = o_ref[0, 0:64, :] * weight
    remote(orecv, orecv, o_s, o_r, up).wait_recv()
    for i in (2, 1, 0):
        weight = jnp.exp2(unpacked(i, 4) - top_m)
        total = total + unpacked(i, 0) * weight
        mixed = mixed + orecv[i].astype(F32) * weight
    mixed = mixed / total
    for k in range(NX):
        cols = mixed[:, 2 * QUARTER * k : 2 * QUARTER * (k + 1)]
        attended = jnp.concatenate([cols[:, 0:QUARTER], cols[:, QUARTER:]], axis=0).T.astype(BF16)
        for h in range(NC):
            asend[NC * k + h] = attended[OWN * h : OWN * (h + 1)]
    arecv[tp] = asend[tp]
    for d in range(1, NT):
        t, device = tp_peer(d)
        go(remote(asend.at[t], arecv.at[tp], a_s, a_r, device))
    loads[6].wait()
    arrived(arecv.at[pl.ds(0, NT - 1)], a_r)
    heads = jnp.concatenate([arecv[t] for t in range(NT)], axis=1)
    writes = []
    for i in range(4):
        cols = slice(512 * i, 512 * (i + 1))
        branch = jnp.dot(heads, wo[:, cols], preferred_element_type=F32)
        result[:, cols] = (
            lat[tp, :, cols].astype(F32) + vecs[2:3, cols] * branch
        ).astype(BF16)
        strip = pl.ds(512 * i, 512)
        write = pltpu.make_async_copy(result.at[:, strip], out.at[:, strip], out_sem.at[i])
        write.start()
        writes.append(write)

    for ref, sem in (
        (mod1.at[pl.ds(0, NZ - 1)], mod1_s),
        (mod2.at[pl.ds(0, NY - 1)], mod2_s),
        (mod3.at[pl.ds(0, NT - 1)], mod3_s),
        (lat.at[pl.ds(0, NT - 1)], lat_s),
        (qraw.at[pl.ds(0, NY - 1)], q_s),
        (kv.at[pl.ds(0, NZ - 1)], kv_s),
        (ctx.at[pl.ds(0, NZ - 1)], ctx_s),
        (osend, o_s),
        (lmsend, lm_s),
        (arecv.at[pl.ds(0, NT - 1)], a_s),
    ):
        remote(ref, ref, sem, sem, up).wait_send()
    for write in writes:
        write.wait()


def on_device(
    latent,
    context,
    condition,
    context_condition,
    norm_gain,
    shift_weight,
    scale_weight,
    gate_weight,
    query_weight,
    key_weight,
    value_weight,
    query_gain,
    key_gain,
    output_weight,
):
    hbm = pl.BlockSpec(memory_space=pl.ANY)
    dma, V = pltpu.SemaphoreType.DMA, pltpu.VMEM
    return pl.pallas_call(
        kernel,
        out_shape=jax.ShapeDtypeStruct((OWN, D), BF16),
        in_specs=[hbm] * 14,
        out_specs=hbm,
        scratch_shapes=[
            V((CTX, D), BF16),
            V((1, D), F32),
            V((1, D), F32),
            V((1, D), F32),
            V((1, HEAD), F32),
            V((1, HEAD), F32),
            V((OWN, D), BF16),
            V((128, 768), BF16),
            V((D, 256), BF16),
            V((128, D), BF16),
            V((1024, D), BF16),
            V((NZ, 8, 256), F32),
            V((NY, 8, 256), F32),
            V((NT, 8, 256), F32),
            V((8, D), F32),
            V((NT, OWN, D), BF16),
            V((QUARTER + CTX, D), BF16),
            V((4, 16, TOK), F32),
            V((NY, NX, HEAD, 2 * QUARTER), BF16),
            V((NY, 2 * HEAD, COLS), BF16),
            V((NZ, 512, 128), BF16),
            V((NZ, TOK, 128), BF16),
            V((NZ, 80, TOK), BF16),
            V((NZ, CTX, 128), BF16),
            V((NZ * CTX, 128), BF16),
            V((80, NZ * CTX), BF16),
            V((NY, 1, COLS), F32),
            V((NY, 80, COLS), F32),
            V((2, TOK, COLS), F32),
            V((2, 1, COLS), F32),
            V((NY - 1, HEAD, COLS), BF16),
            V((NY - 1, 8, 256), F32),
            V((NY - 1, HEAD, COLS), BF16),
            V((NY - 1, 8, 256), F32),
            V((NT, OWN, 128), BF16),
            V((NT, OWN, 128), BF16),
            dma((14,)),
            dma((4,)),
            dma,
            dma,
            dma,
            dma,
            dma,
            dma,
            dma,
            dma((4,)),
            dma((4,)),
            dma((7,)),
            dma,
            dma((NY - 1,)),
            dma,
            dma((NZ - 1, NX)),
            dma,
            dma,
            dma,
            dma,
            dma,
            dma,
            dma,
            dma,
        ],
        compiler_params=pltpu.CompilerParams(
            collective_id=0, has_side_effects=True, vmem_limit_bytes=60 * 2**20
        ),
    )(
        latent,
        context,
        condition.reshape(1, D),
        context_condition.reshape(1, D),
        norm_gain.reshape(1, D),
        shift_weight,
        scale_weight,
        gate_weight,
        query_weight,
        key_weight.T,
        value_weight.T,
        query_gain.reshape(1, HEAD),
        key_gain.reshape(1, HEAD),
        output_weight,
    )


def solution(mesh):
    split = Mesh(mesh.devices.reshape(NZ, NY, NX, NC), AXES)
    seq, tp, everything = ("z", "y"), ("x", "c"), AXES
    return jax.shard_map(
        on_device,
        mesh=split,
        in_specs=(
            P(everything, None),
            P(seq, None),
            P(),
            P(),
            P(),
            P(seq, tp),
            P(seq, tp),
            P(seq, tp),
            P(None, tp),
            P(None, tp),
            P(None, tp),
            P(),
            P(),
            P(),
        ),
        out_specs=P(everything, None),
        check_vma=False,
    )
```

time: 74.5 us -> 61 us (0.82)
  Pallas kernels: 68.7 us -> 59.2 us
  local copies, waits for them, and re-layouts: 5.59 us -> 1.67 us
    pallas_call x1, Pallas kernels: 68.7 us -> 59.2 us  [on_device(): pl.pallas_call(kernel, out_shape=jax.ShapeDtypeStruct((OWN, D), BF16), in...]
    unnamed x3 -> x1, local copies, waits for them, and re-layouts: 5.59 us -> 1.67 us
where the time goes in v2:
time: 61 us; the launch traced here: 60.8 us
  Pallas kernels  59.2 us (97%)
  local copies, waits for them, and re-layouts  1.67 us (3%)
    pallas_call x1, Pallas kernels, on_device(): pl.pallas_call(kernel, out_shape=jax.ShapeDtypeStruct((OWN, D), BF16), in...  59.2 us
    unnamed x1, local copies, waits for them, and re-layouts  1.67 us

profile of v2, /device:TPU:1, one launch (start us, length us, event | category | flops | bytes accessed | tf_op | source)
XLA Modules:
  0.0 60.8 jit_solution(1373058023858584329)
XLA Ops:
  0.0 59.2 %shard_map.136 = bf16[64,2048]{1,0:T(8,128)(2,1)} custom-call(bf16[64,2048]{1,0:T(8,128)(2,1)} %latent.1, bf16[16,2048]{1,0:T(8,128)(2,1)} %context_in.1, f32[1,2048]{1,0:T(1,128)} %bitcast.9, f32[1,2048]{1,0:T(1,128)} %bitcast.10, f32[1,2048]{1,0:T(1,128)} %bitcast.11, bf16[64,256]{1,0:T(8,128)(2,1)} %shift_w.1, bf16[64,256]{1,0:T(8,128)(2,1)} %scale_w.1, ...), custom_call_target="tpu_custom_call" | custom-call | tf_op jit(solution)/shard_map/pallas_call | solution.py:644
  59.2 1.7 %copy.16 = bf16[64,2048]{1,0:T(8,128)(2,1)} copy(bf16[64,2048]{1,0:T(8,128)(2,1)} %shard_map.136) | data formatting | bytes 524288

commit v3 on v2

--- a/solution.py
+++ b/solution.py
@@ -62,7 +62,6 @@
     norm_gain,
     query_gain,
     key_gain,
-    result,
     wmod,
     wcat,
     kvw,
@@ -72,6 +71,7 @@
     mod3,
     vecs,
     lat,
+    scales,
     hid,
     tables,
     qraw,
@@ -85,15 +85,16 @@
     m_ref,
     o_ref,
     s_ref,
+    cs_ref,
     mx_ref,
     osend,
     lmsend,
     orecv,
     lmrecv,
+    orelay,
     asend,
     arecv,
     local_sem,
-    out_sem,
     mod1_s,
     mod1_r,
     mod2_s,
@@ -112,6 +113,7 @@
     ctx_r,
     o_s,
     o_r,
+    or_r,
     lm_s,
     lm_r,
     a_s,
@@ -268,6 +270,28 @@
     arrived(lat_half(1, top), lx_r.at[3])
     go(remote(lat_half(1, top), lat_half(1, top), lat_s, lc_r.at[4], mate))
 
+    def mate_block(d):
+        return at_x(d) * NC + 1 - c
+
+    def row_scale(rows_):
+        wide = rows_.astype(F32)
+        return lax.rsqrt(jnp.mean(wide * wide, axis=1, keepdims=True) + EPS)
+
+    def measure_rows(i):
+        for k in range(NC):
+            block = at_x(ORDER[i]) * NC + k
+            scales[block] = jnp.broadcast_to(row_scale(lat[block]), (OWN, 128))
+
+    arrived(lat.at[mate_block(0)], lc_r.at[0])
+    measure_rows(0)
+    arrived(lat.at[mate_block(-1), top], lc_r.at[1])
+    arrived(lat.at[mate_block(-1), low], lc_r.at[3])
+    measure_rows(1)
+    arrived(lat.at[mate_block(1), low], lc_r.at[2])
+    arrived(lat.at[mate_block(1), top], lc_r.at[4])
+    measure_rows(2)
+    context_scale = row_scale(context[...])
+
     arrived(mod3.at[pl.ds(0, NT - 1)], mod3_r)
     vec = jnp.concatenate([mod3[t] for t in range(NT)], axis=1)
     vecs[0:1] = norm_gain[...] * (1.0 + vec[1:2])
@@ -275,13 +299,6 @@
     vecs[2:3] = vec[2:3]
     vecs[3:4] = norm_gain[...] * (1.0 + vec[4:5])
     vecs[4:5] = vec[3:4]
-
-    def modulated(rows_, gain, shift):
-        wide = rows_.astype(F32)
-        mean = jnp.mean(wide * wide, axis=1, keepdims=True)
-        return ((wide * lax.rsqrt(mean + EPS)) * gain + shift).astype(BF16)
-
-    hid[QUARTER:, :] = modulated(context[...], vecs[3:4], vecs[4:5])
 
     def normed(field, gain):
         mean = jnp.mean(field * field, axis=0, keepdims=True)
@@ -307,21 +324,37 @@
         dst = kv.at[slot, part_of(i)]
         remote(dst, dst, kv_s, kv_r.at[slot - 1, i], up).wait_recv()
 
-    def process(i):
+    def process(quarters):
+        for n, i in enumerate(quarters):
+            xb = at_x(ORDER[i])
+            for k in range(NC):
+                block = xb * NC + k
+                if i < 3:
+                    scale = scales[block, :, 0:1]
+                else:
+                    scale = row_scale(lat[block])
+                hid[QUARTER * n + OWN * k : QUARTER * n + OWN * (k + 1), :] = (
+                    lat[block].astype(F32) * scale * vecs[0:1] + vecs[1:2]
+                ).astype(BF16)
+        many = QUARTER * len(quarters)
+        if quarters[0] == 0:
+            hid[many : many + CTX, :] = (
+                context[...].astype(F32) * context_scale * vecs[3:4] + vecs[4:5]
+            ).astype(BF16)
+            many += CTX
+        all_projected = jnp.dot(hid[0:many], wcat[...], preferred_element_type=F32)
+        for n, i in enumerate(quarters):
+            share_out(i, all_projected[QUARTER * n : QUARTER * (n + 1)].T)
+        if quarters[0] == 0:
+            cp = all_projected[QUARTER : QUARTER + CTX]
+            ck = cp[:, 128:192]
+            ck = ck * lax.rsqrt(jnp.mean(ck * ck, axis=1, keepdims=True) + EPS) * key_gain[...]
+            ctx[z] = jnp.concatenate([ck, cp[:, 192:256]], axis=1).astype(BF16)
+            for d in range(1, NZ):
+                go(remote(ctx.at[z], ctx.at[z], ctx_s, ctx_r, {"z": at_z(d)}))
+
+    def share_out(i, turned):
         xb = at_x(ORDER[i])
-
-        def normalize(k, carry):
-            hid[pl.ds(pl.multiple_of(k * 32, 32), 32), :] = modulated(
-                lat[xb * NC + k // 2, pl.ds(pl.multiple_of(lax.rem(k, 2) * 32, 32), 32)],
-                vecs[0:1],
-                vecs[1:2],
-            )
-            return carry
-
-        lax.fori_loop(0, QUARTER // 32, normalize, 0)
-        many = QUARTER + CTX if i == 0 else QUARTER
-        projected = jnp.dot(hid[0:many], wcat[...], preferred_element_type=F32)
-        turned = projected[0:QUARTER].T
         lanes = pl.ds(pl.multiple_of(xb * QUARTER, QUARTER), QUARTER)
         cr, sr, cc, sc = (tables[k, :, lanes] for k in range(4))
 
@@ -341,7 +374,7 @@
         for h in range(2):
             q = rotated(normed(turned[64 * h : 64 * h + 64], query_column))
             qraw[0, xb, :, QUARTER * h : QUARTER * (h + 1)] = q.astype(BF16)
-        for g in range(1, NY):
+        for g in (1, 2):
             go(
                 remote(
                     qraw.at[0, xb],
@@ -351,19 +384,8 @@
                     y_of[g],
                 )
             )
-        if i == 0:
-            cp = projected[QUARTER : QUARTER + CTX]
-            ck = cp[:, 128:192]
-            ck = ck * lax.rsqrt(jnp.mean(ck * ck, axis=1, keepdims=True) + EPS) * key_gain[...]
-            ctx[z] = jnp.concatenate([ck, cp[:, 192:256]], axis=1).astype(BF16)
-            for d in range(1, NZ):
-                go(remote(ctx.at[z], ctx.at[z], ctx_s, ctx_r, {"z": at_z(d)}))
-
-    def mate_block(d):
-        return at_x(d) * NC + 1 - c
-
-    arrived(lat.at[mate_block(0)], lc_r.at[0])
-    process(0)
+
+    process((0,))
 
     arrived(lat_half(2, piece[0]), lf_r.at[0])
     arrived(lat_half(2, piece[1]), lf_r.at[1])
@@ -372,18 +394,12 @@
     arrived(lat_half(2, piece[3]), lf_r.at[3])
     go(remote(lat_half(2, low), lat_half(2, low), lat_s, lc_r.at[6], mate))
 
-    arrived(lat.at[mate_block(-1), top], lc_r.at[1])
-    arrived(lat.at[mate_block(-1), low], lc_r.at[3])
-    process(1)
-
-    arrived(lat.at[mate_block(1), low], lc_r.at[2])
-    arrived(lat.at[mate_block(1), top], lc_r.at[4])
-    process(2)
+    process((1, 2))
 
     arrived(lat.at[mate_block(2), top], lc_r.at[5])
     arrived(lat.at[mate_block(2), low], lc_r.at[6])
 
-    process(3)
+    process((3,))
 
     def prepare_queries(g):
         for k in range(NX):
@@ -412,11 +428,11 @@
     def tile_of(t):
         w, v = t - 1 + 6, t - 19 + 20
         slot = pick(
-            [(t < 1, 0), (t < 5, w // 2 - 3), (t < 7, t - 5), (t < 19, w // 3 - 2), (t < 25, 6 + lax.rem(v, 2))],
+            [(t < 1, 0), (t < 9, w // 2 - 3), (t < 13, t - 9), (t < 19, w // 3 - 2), (t < 25, 6 + lax.rem(v, 2))],
             t - 24,
         )
         group = pick(
-            [(t < 1, 0), (t < 5, 1 + lax.rem(w, 2)), (t < 7, 3), (t < 19, 1 + lax.rem(w, 3)), (t < 25, 13 - v // 2)],
+            [(t < 1, 0), (t < 9, 1 + lax.rem(w, 2)), (t < 13, 3), (t < 19, 1 + lax.rem(w, 3)), (t < 25, 13 - v // 2)],
             0,
         )
         return slot, group
@@ -447,15 +463,28 @@
         for cols in strips:
             absorb_strip(tile_of(t), side, cols)
 
+    def score_context(g):
+        for cols in strips:
+            s = jnp.dot(ckk[...], qhl[g, :, cols], preferred_element_type=F32)
+            cs_ref[g, :, cols] = s + math.log2(TOK / (2.0 * CTX))
+
     def absorb_context(g):
-        s = jnp.dot(ckk[...], qhl[g], preferred_element_type=F32) + math.log2(TOK / (2.0 * CTX))
-        old = m_ref[g]
-        new = jnp.maximum(old, jnp.max(s, axis=0, keepdims=True))
-        p = jnp.exp2(s - new).astype(BF16)
-        m_ref[g] = new
-        o_ref[g] = o_ref[g] * jnp.exp2(old - new) + jnp.dot(
-            cvt[...], p, preferred_element_type=F32
-        )
+        for cols in strips:
+            s = cs_ref[g, :, cols]
+            old = m_ref[g, :, cols]
+            new = jnp.maximum(old, jnp.max(s, axis=0, keepdims=True))
+            p = jnp.exp2(s - new).astype(BF16)
+            m_ref[g, :, cols] = new
+            o_ref[g, :, cols] = o_ref[g, :, cols] * jnp.exp2(old - new) + jnp.dot(
+                cvt[...], p, preferred_element_type=F32
+            )
+
+    halves = (pl.ds(0, HEAD // 2), pl.ds(HEAD // 2, HEAD // 2))
+
+    def relay_out():
+        for k in range(2):
+            remote(orelay.at[k], orelay.at[k], o_s, or_r.at[k], up).wait_recv()
+            remote(orelay.at[k], orecv.at[2, halves[k]], o_s, o_r, y_of[k + 1]).start()
 
     def send_out(g):
         osend[g - 1] = o_ref[g, 0:64, :].astype(BF16)
@@ -463,7 +492,11 @@
             lmsend[g - 1, i : i + 1, :] = o_ref[g, 64:65, 256 * i : 256 * (i + 1)]
             lmsend[g - 1, 4 + i : 5 + i, :] = m_ref[g, :, 256 * i : 256 * (i + 1)]
         to = there[g] - 1
-        remote(osend.at[g - 1], orecv.at[to], o_s, o_r, y_of[g]).start()
+        if g == 3:
+            for k in range(2):
+                remote(osend.at[2, halves[k]], orelay.at[k], o_s, or_r.at[k], y_of[k + 1]).start()
+        else:
+            remote(osend.at[g - 1], orecv.at[to], o_s, o_r, y_of[g]).start()
         remote(lmsend.at[g - 1], lmrecv.at[to], lm_s, lm_r, y_of[g]).start()
 
     def pass_on(i):
@@ -478,6 +511,13 @@
     absorb(0, 0)
 
     pass_on(1)
+    arrived(ctx.at[pl.ds(0, NZ - 1)], ctx_r)
+    every = ctx[...].reshape(NZ * CTX, 128)
+    ckk[...] = jnp.concatenate([every[:, 0:64], every[:, 0:64]], axis=1)
+    cvt[0:64, :] = every.astype(F32).T[64:128].astype(BF16)
+    score_context(0)
+    absorb_context(0)
+
     pass_on(2)
     pass_on(3)
     prepare_keys(1)
@@ -488,14 +528,12 @@
         prepare_queries(g)
 
     queries_arrived(1)
+    go(remote(qraw.at[1, pl.ds(0, 2)], qraw.at[3, pl.ds(0, 2)], q_s, q_r.at[2], y_of[2]))
+    score(1, 1)
     queries_arrived(2)
-    score(1, 1)
+    go(remote(qraw.at[2, pl.ds(2, 2)], qraw.at[3, pl.ds(2, 2)], q_s, q_r.at[2], y_of[1]))
 
     def body(j, carry):
-        @pl.when(j == 1)
-        def _():
-            queries_arrived(3)
-
         @pl.when(j == 1)
         def _():
             for slot in (3, 4):
@@ -504,17 +542,15 @@
 
         @pl.when(j == 2)
         def _():
-            for i in (1, 2):
+            for i in (1, 2, 3):
                 for slot in (3, 4):
                     kv_arrived(slot, i)
                     fwd(slot, i)
+            prepare_keys(3)
 
         @pl.when(j == 3)
         def _():
-            for slot in (3, 4):
-                kv_arrived(slot, 3)
-                fwd(slot, 3)
-            prepare_keys(3)
+            queries_arrived(3)
             prepare_keys(4)
 
         @pl.when(j == 5)
@@ -538,15 +574,15 @@
             for i in range(NX):
                 kv_arrived(7, i)
             prepare_keys(7)
-            arrived(ctx.at[pl.ds(0, NZ - 1)], ctx_r)
-            every = ctx[...].reshape(NZ * CTX, 128)
-            ckk[...] = jnp.concatenate([every[:, 0:64], every[:, 0:64]], axis=1)
-            cvt[0:64, :] = every.astype(F32).T[64:128].astype(BF16)
-            for g in range(NY):
+            for g in (1, 2, 3):
+                score_context(g)
+            for g in (1, 2, 3):
                 absorb_context(g)
 
         for k, g in ((10, 3), (11, 2), (12, 1)):
             pl.when(j == k)(functools.partial(send_out, g))
+
+        pl.when(j == tiles // 2 - 3)(relay_out)
 
         now = tile_of(2 * j + 1)
         for u in range(2):
@@ -594,17 +630,12 @@
     loads[6].wait()
     arrived(arecv.at[pl.ds(0, NT - 1)], a_r)
     heads = jnp.concatenate([arecv[t] for t in range(NT)], axis=1)
-    writes = []
     for i in range(4):
         cols = slice(512 * i, 512 * (i + 1))
         branch = jnp.dot(heads, wo[:, cols], preferred_element_type=F32)
-        result[:, cols] = (
+        out[:, cols] = (
             lat[tp, :, cols].astype(F32) + vecs[2:3, cols] * branch
         ).astype(BF16)
-        strip = pl.ds(512 * i, 512)
-        write = pltpu.make_async_copy(result.at[:, strip], out.at[:, strip], out_sem.at[i])
-        write.start()
-        writes.append(write)
 
     for ref, sem in (
         (mod1.at[pl.ds(0, NZ - 1)], mod1_s),
@@ -614,13 +645,11 @@
         (qraw.at[pl.ds(0, NY - 1)], q_s),
         (kv.at[pl.ds(0, NZ - 1)], kv_s),
         (ctx.at[pl.ds(0, NZ - 1)], ctx_s),
-        (osend, o_s),
+        (qraw, o_s),
         (lmsend, lm_s),
         (arecv.at[pl.ds(0, NT - 1)], a_s),
     ):
         remote(ref, ref, sem, sem, up).wait_send()
-    for write in writes:
-        write.wait()
 
 
 def on_device(
@@ -643,9 +672,9 @@
     dma, V = pltpu.SemaphoreType.DMA, pltpu.VMEM
     return pl.pallas_call(
         kernel,
-        out_shape=jax.ShapeDtypeStruct((OWN, D), BF16),
+        out_shape=pltpu.VMEM((OWN, D), BF16),
         in_specs=[hbm] * 14,
-        out_specs=hbm,
+        out_specs=pl.BlockSpec(memory_space=pltpu.VMEM),
         scratch_shapes=[
             V((CTX, D), BF16),
             V((1, D), F32),
@@ -653,7 +682,6 @@
             V((1, D), F32),
             V((1, HEAD), F32),
             V((1, HEAD), F32),
-            V((OWN, D), BF16),
             V((128, 768), BF16),
             V((D, 256), BF16),
             V((128, D), BF16),
@@ -663,7 +691,8 @@
             V((NT, 8, 256), F32),
             V((8, D), F32),
             V((NT, OWN, D), BF16),
-            V((QUARTER + CTX, D), BF16),
+            V((NT, OWN, 128), F32),
+            V((2 * QUARTER, D), BF16),
             V((4, 16, TOK), F32),
             V((NY, NX, HEAD, 2 * QUARTER), BF16),
             V((NY, 2 * HEAD, COLS), BF16),
@@ -676,15 +705,16 @@
             V((NY, 1, COLS), F32),
             V((NY, 80, COLS), F32),
             V((2, TOK, COLS), F32),
+            V((NY, NZ * CTX, COLS), F32),
             V((2, 1, COLS), F32),
             V((NY - 1, HEAD, COLS), BF16),
             V((NY - 1, 8, 256), F32),
             V((NY - 1, HEAD, COLS), BF16),
             V((NY - 1, 8, 256), F32),
+            V((2, HEAD // 2, COLS), BF16),
             V((NT, OWN, 128), BF16),
             V((NT, OWN, 128), BF16),
             dma((14,)),
-            dma((4,)),
             dma,
             dma,
             dma,
@@ -703,6 +733,7 @@
             dma,
             dma,
             dma,
+            dma((2,)),
             dma,
             dma,
             dma,

time: 61 us -> 57.1 us (0.936)
  Pallas kernels: 59.2 us -> 56.3 us
  local copies, waits for them, and re-layouts: 1.67 us -> 0.71 us
    pallas_call x1, Pallas kernels: 59.2 us -> 56.3 us  [on_device(): pl.pallas_call(kernel, out_shape=pltpu.VMEM((OWN, D), BF16), in_specs=[hb...]
    unnamed x1, local copies, waits for them, and re-layouts: 1.67 us -> 0.71 us
where the time goes in v3:
time: 57.1 us; the launch traced here: 57 us
  Pallas kernels  56.3 us (99%)
  local copies, waits for them, and re-layouts  0.71 us (1%)
    pallas_call x1, Pallas kernels, on_device(): pl.pallas_call(kernel, out_shape=pltpu.VMEM((OWN, D), BF16), in_specs=[hb...  56.3 us

profile of v3, /device:TPU:1, one launch (start us, length us, event | category | flops | bytes accessed | tf_op | source)
XLA Modules:
  0.0 57.0 jit_solution(10224077513231270563)
XLA Ops:
  0.0 56.3 %shard_map.136 = bf16[64,2048]{1,0:T(8,128)(2,1)S(1)} custom-call(bf16[64,2048]{1,0:T(8,128)(2,1)} %latent.1, bf16[16,2048]{1,0:T(8,128)(2,1)} %context_in.1, f32[1,2048]{1,0:T(1,128)} %bitcast.9, f32[1,2048]{1,0:T(1,128)} %bitcast.10, f32[1,2048]{1,0:T(1,128)} %bitcast.11, bf16[64,256]{1,0:T(8,128)(2,1)} %shift_w.1, bf16[64,256]{1,0:T(8,128)(2,1)} %scale_w.1, ...), custom_call_target="tpu_custom_call" | custom-call | tf_op jit(solution)/shard_map/pallas_call | solution.py:673
  56.3 0.7 %copy.16 = bf16[64,2048]{1,0:T(8,128)(2,1)} copy(bf16[64,2048]{1,0:T(8,128)(2,1)S(1)} %shard_map.136) | data formatting | bytes 524288

commit v4 on v3

--- a/solution.py
+++ b/solution.py
@@ -80,12 +80,9 @@
     kk,
     vt,
     ctx,
-    ckk,
-    cvt,
     m_ref,
     o_ref,
     s_ref,
-    cs_ref,
     mx_ref,
     osend,
     lmsend,
@@ -111,6 +108,8 @@
     kv_r,
     ctx_s,
     ctx_r,
+    cy_s,
+    cy_r,
     o_s,
     o_r,
     or_r,
@@ -233,7 +232,6 @@
     for r in range(NZ):
         vt[r, 64:80, :] = jnp.ones((16, TOK), BF16)
     key_column, query_column = column(key_gain[...]), column(query_gain[...])
-    cvt[64:80, :] = jnp.ones((16, CTX * NZ), BF16)
     m_ref[...] = jnp.full(m_ref.shape, -1e30, F32)
     o_ref[...] = jnp.zeros(o_ref.shape, F32)
 
@@ -349,9 +347,9 @@
             cp = all_projected[QUARTER : QUARTER + CTX]
             ck = cp[:, 128:192]
             ck = ck * lax.rsqrt(jnp.mean(ck * ck, axis=1, keepdims=True) + EPS) * key_gain[...]
-            ctx[z] = jnp.concatenate([ck, cp[:, 192:256]], axis=1).astype(BF16)
+            ctx[y, z] = jnp.concatenate([ck, cp[:, 192:256]], axis=1).astype(BF16)
             for d in range(1, NZ):
-                go(remote(ctx.at[z], ctx.at[z], ctx_s, ctx_r, {"z": at_z(d)}))
+                go(remote(ctx.at[y, z], ctx.at[y, z], ctx_s, ctx_r, {"z": at_z(d)}))
 
     def share_out(i, turned):
         xb = at_x(ORDER[i])
@@ -428,11 +426,11 @@
     def tile_of(t):
         w, v = t - 1 + 6, t - 19 + 20
         slot = pick(
-            [(t < 1, 0), (t < 9, w // 2 - 3), (t < 13, t - 9), (t < 19, w // 3 - 2), (t < 25, 6 + lax.rem(v, 2))],
+            [(t < 1, 0), (t < 11, w // 2 - 3), (t < 16, t - 11), (t < 19, 5), (t < 25, 6 + lax.rem(v, 2))],
             t - 24,
         )
         group = pick(
-            [(t < 1, 0), (t < 9, 1 + lax.rem(w, 2)), (t < 13, 3), (t < 19, 1 + lax.rem(w, 3)), (t < 25, 13 - v // 2)],
+            [(t < 1, 0), (t < 11, 1 + lax.rem(w, 2)), (t < 16, 3), (t < 19, t - 15), (t < 25, 13 - v // 2)],
             0,
         )
         return slot, group
@@ -462,22 +460,6 @@
     def absorb(t, side):
         for cols in strips:
             absorb_strip(tile_of(t), side, cols)
-
-    def score_context(g):
-        for cols in strips:
-            s = jnp.dot(ckk[...], qhl[g, :, cols], preferred_element_type=F32)
-            cs_ref[g, :, cols] = s + math.log2(TOK / (2.0 * CTX))
-
-    def absorb_context(g):
-        for cols in strips:
-            s = cs_ref[g, :, cols]
-            old = m_ref[g, :, cols]
-            new = jnp.maximum(old, jnp.max(s, axis=0, keepdims=True))
-            p = jnp.exp2(s - new).astype(BF16)
-            m_ref[g, :, cols] = new
-            o_ref[g, :, cols] = o_ref[g, :, cols] * jnp.exp2(old - new) + jnp.dot(
-                cvt[...], p, preferred_element_type=F32
-            )
 
     halves = (pl.ds(0, HEAD // 2), pl.ds(HEAD // 2, HEAD // 2))
 
@@ -511,12 +493,9 @@
     absorb(0, 0)
 
     pass_on(1)
-    arrived(ctx.at[pl.ds(0, NZ - 1)], ctx_r)
-    every = ctx[...].reshape(NZ * CTX, 128)
-    ckk[...] = jnp.concatenate([every[:, 0:64], every[:, 0:64]], axis=1)
-    cvt[0:64, :] = every.astype(F32).T[64:128].astype(BF16)
-    score_context(0)
-    absorb_context(0)
+    arrived(ctx.at[0, pl.ds(0, NZ - 1)], ctx_r)
+    for g in range(1, NY):
+        go(remote(ctx.at[y], ctx.at[y], cy_s, cy_r, y_of[g]))
 
     pass_on(2)
     pass_on(3)
@@ -533,74 +512,82 @@
     queries_arrived(2)
     go(remote(qraw.at[2, pl.ds(2, 2)], qraw.at[3, pl.ds(2, 2)], q_s, q_r.at[2], y_of[1]))
 
-    def body(j, carry):
-        @pl.when(j == 1)
-        def _():
-            for slot in (3, 4):
-                kv_arrived(slot, 0)
-                fwd(slot, 0)
-
-        @pl.when(j == 2)
-        def _():
-            for i in (1, 2, 3):
-                for slot in (3, 4):
-                    kv_arrived(slot, i)
-                    fwd(slot, i)
-            prepare_keys(3)
-
-        @pl.when(j == 3)
-        def _():
-            queries_arrived(3)
-            prepare_keys(4)
-
-        @pl.when(j == 5)
-        def _():
-            for i in (0, 1):
-                kv_arrived(5, i)
-                fwd(5, i)
-                kv_arrived(6, i)
-
-        @pl.when(j == 6)
-        def _():
-            for i in (2, 3):
-                kv_arrived(6, i)
-                fwd(6, i)
-                kv_arrived(5, i)
-            prepare_keys(5)
-            prepare_keys(6)
-
-        @pl.when(j == 9)
-        def _():
-            for i in range(NX):
-                kv_arrived(7, i)
-            prepare_keys(7)
-            for g in (1, 2, 3):
-                score_context(g)
-            for g in (1, 2, 3):
-                absorb_context(g)
-
-        for k, g in ((10, 3), (11, 2), (12, 1)):
-            pl.when(j == k)(functools.partial(send_out, g))
-
-        pl.when(j == tiles // 2 - 3)(relay_out)
-
-        now = tile_of(2 * j + 1)
-        for u in range(2):
-            t = 2 * j + 1 + u
-            side = (u + 1) % 2
-            following = tile_of(t + 1)
-            for cols in strips:
-                score_strip(following, 1 - side, cols)
-                absorb_strip(now, side, cols)
-            now = following
-        return carry
-
     def fwd(slot, i):
         copy = kv_copy(slot, min(slot + 2, 7), i)
         copy.start()
 
-    lax.fori_loop(0, tiles // 2 - 1, body, 0)
-    absorb(tiles - 1, 1)
+    def take(*chunks):
+        for slot, i, forward in chunks:
+            kv_arrived(slot, i)
+            if forward:
+                fwd(slot, i)
+
+    def far_keys_0():
+        take((3, 0, True), (4, 0, True), (3, 1, True), (4, 1, True))
+
+    def far_keys_1():
+        take((3, 2, True), (4, 2, True), (3, 3, True), (4, 3, True))
+        prepare_keys(3)
+        prepare_keys(4)
+
+    def far_keys_2():
+        queries_arrived(3)
+        take((5, 0, True), (5, 1, True), (6, 0, False), (6, 1, False), (6, 2, True), (6, 3, True))
+
+    def far_keys_3():
+        take((5, 2, False), (5, 3, False))
+        prepare_keys(5)
+        prepare_keys(6)
+
+    def context_keys():
+        arrived(ctx.at[pl.ds(0, NY - 1)], cy_r)
+        every = ctx[...].reshape(TOK, 128)
+        kk[NZ] = jnp.concatenate([every[:, 0:64], every[:, 0:64]], axis=1)
+        weight = TOK / (2.0 * CTX)
+        vt[NZ, 0:64, :] = (every.astype(F32).T[64:128] * weight).astype(BF16)
+        vt[NZ, 64:80, :] = jnp.full((16, TOK), weight, BF16)
+
+    def farthest_keys():
+        take((7, 0, False), (7, 1, False), (7, 2, False), (7, 3, False))
+        prepare_keys(7)
+
+    def tiles_from(start, stop, each, events):
+        def body(j, carry):
+            for k, event in events:
+                pl.when(j == k)(event)
+            now = tile_of(start + each * j)
+            for u in range(each):
+                side = (start + u) % 2
+                following = tile_of(start + each * j + u + 1)
+                for cols in strips:
+                    score_strip(following, 1 - side, cols)
+                    absorb_strip(now, side, cols)
+                now = following
+            return carry
+
+        lax.fori_loop(0, (stop - start) // each, body, 0)
+
+    tiles_from(
+        1, 21, 4, ((0, far_keys_0), (1, far_keys_1), (2, far_keys_2), (3, far_keys_3), (4, farthest_keys))
+    )
+
+    tiles_from(
+        21,
+        31,
+        2,
+        (
+            (0, functools.partial(send_out, 3)),
+            (1, functools.partial(send_out, 2)),
+            (2, functools.partial(send_out, 1)),
+            (3, relay_out),
+            (4, context_keys),
+        ),
+    )
+
+    for cols in strips:
+        score_strip(tile_of(tiles), 0, cols)
+        absorb_strip(tile_of(tiles - 1), 1, cols)
+    absorb(tiles, 0)
 
     def unpacked(i, first):
         return jnp.concatenate([lmrecv[i, first + k : first + k + 1, :] for k in range(4)], axis=1)
@@ -644,7 +631,8 @@
         (lat.at[pl.ds(0, NT - 1)], lat_s),
         (qraw.at[pl.ds(0, NY - 1)], q_s),
         (kv.at[pl.ds(0, NZ - 1)], kv_s),
-        (ctx.at[pl.ds(0, NZ - 1)], ctx_s),
+        (ctx.at[0, pl.ds(0, NZ - 1)], ctx_s),
+        (ctx.at[pl.ds(0, NY - 1)], cy_s),
         (qraw, o_s),
         (lmsend, lm_s),
         (arecv.at[pl.ds(0, NT - 1)], a_s),
@@ -697,15 +685,12 @@
             V((NY, NX, HEAD, 2 * QUARTER), BF16),
             V((NY, 2 * HEAD, COLS), BF16),
             V((NZ, 512, 128), BF16),
-            V((NZ, TOK, 128), BF16),
-            V((NZ, 80, TOK), BF16),
-            V((NZ, CTX, 128), BF16),
-            V((NZ * CTX, 128), BF16),
-            V((80, NZ * CTX), BF16),
+            V((NZ + 1, TOK, 128), BF16),
+            V((NZ + 1, 80, TOK), BF16),
+            V((NY, NZ, CTX, 128), BF16),
             V((NY, 1, COLS), F32),
             V((NY, 80, COLS), F32),
             V((2, TOK, COLS), F32),
-            V((NY, NZ * CTX, COLS), F32),
             V((2, 1, COLS), F32),
             V((NY - 1, HEAD, COLS), BF16),
             V((NY - 1, 8, 256), F32),
@@ -729,6 +714,8 @@
             dma((NY - 1,)),
             dma,
             dma((NZ - 1, NX)),
+            dma,
+            dma,
             dma,
             dma,
             dma,

time: 57.1 us -> 56 us (0.981)
  Pallas kernels: 56.3 us -> 55.2 us
    pallas_call x1, Pallas kernels: 56.3 us -> 55.2 us  [on_device(): pl.pallas_call(kernel, out_shape=pltpu.VMEM((OWN, D), BF16), in_specs=[hb...]
where the time goes in v4:
time: 56 us; the launch traced here: 55.9 us
  Pallas kernels  55.2 us (99%)
  local copies, waits for them, and re-layouts  0.71 us (1%)
    pallas_call x1, Pallas kernels, on_device(): pl.pallas_call(kernel, out_shape=pltpu.VMEM((OWN, D), BF16), in_specs=[hb...  55.2 us

profile of v4, /device:TPU:1, one launch (start us, length us, event | category | flops | bytes accessed | tf_op | source)
XLA Modules:
  0.0 55.9 jit_solution(8301821686129471162)
XLA Ops:
  0.0 55.2 %shard_map.136 = bf16[64,2048]{1,0:T(8,128)(2,1)S(1)} custom-call(bf16[64,2048]{1,0:T(8,128)(2,1)} %latent.1, bf16[16,2048]{1,0:T(8,128)(2,1)} %context_in.1, f32[1,2048]{1,0:T(1,128)} %bitcast.9, f32[1,2048]{1,0:T(1,128)} %bitcast.10, f32[1,2048]{1,0:T(1,128)} %bitcast.11, bf16[64,256]{1,0:T(8,128)(2,1)} %shift_w.1, bf16[64,256]{1,0:T(8,128)(2,1)} %scale_w.1, ...), custom_call_target="tpu_custom_call" | custom-call | tf_op jit(solution)/shard_map/pallas_call | solution.py:661
  55.2 0.7 %copy.16 = bf16[64,2048]{1,0:T(8,128)(2,1)} copy(bf16[64,2048]{1,0:T(8,128)(2,1)S(1)} %shard_map.136) | data formatting | bytes 524288

commit v5 on v4

--- a/solution.py
+++ b/solution.py
@@ -523,10 +523,11 @@
                 fwd(slot, i)
 
     def far_keys_0():
-        take((3, 0, True), (4, 0, True), (3, 1, True), (4, 1, True))
+        take((3, 0, True), (4, 0, True))
 
     def far_keys_1():
-        take((3, 2, True), (4, 2, True), (3, 3, True), (4, 3, True))
+        for i in (1, 2, 3):
+            take((3, i, True), (4, i, True))
         prepare_keys(3)
         prepare_keys(4)
 

time: 56 us -> 55.7 us (level)
  no operation moved by 1% of the time
where the time goes in v5:
time: 55.7 us; the launch traced here: 55.6 us
  Pallas kernels  54.9 us (99%)
  local copies, waits for them, and re-layouts  0.71 us (1%)
    pallas_call x1, Pallas kernels, on_device(): pl.pallas_call(kernel, out_shape=pltpu.VMEM((OWN, D), BF16), in_specs=[hb...  54.9 us

profile of v5, /device:TPU:1, one launch (start us, length us, event | category | flops | bytes accessed | tf_op | source)
XLA Modules:
  0.0 55.6 jit_solution(17170058316339088847)
XLA Ops:
  0.0 54.9 %shard_map.136 = bf16[64,2048]{1,0:T(8,128)(2,1)S(1)} custom-call(bf16[64,2048]{1,0:T(8,128)(2,1)} %latent.1, bf16[16,2048]{1,0:T(8,128)(2,1)} %context_in.1, f32[1,2048]{1,0:T(1,128)} %bitcast.9, f32[1,2048]{1,0:T(1,128)} %bitcast.10, f32[1,2048]{1,0:T(1,128)} %bitcast.11, bf16[64,256]{1,0:T(8,128)(2,1)} %shift_w.1, bf16[64,256]{1,0:T(8,128)(2,1)} %scale_w.1, ...), custom_call_target="tpu_custom_call" | custom-call | tf_op jit(solution)/shard_map/pallas_call | solution.py:662
  54.9 0.7 %copy.16 = bf16[64,2048]{1,0:T(8,128)(2,1)} copy(bf16[64,2048]{1,0:T(8,128)(2,1)S(1)} %shard_map.136) | data formatting | bytes 524288
